TPU v7x, 32 devices: a whole 2x2x4 slice. The times are simulated.
32 devices in a mesh: sp: 4 (over y, x), tp: 8 (over z, core).
Axes of the slice: x: 2, y: 2, z: 4, core: 2. Of those that a mesh axis runs over, the one named last changes fastest.
Arguments:
- gate_b: bfloat16 [2048, 1024], P('sp', 'tp'), may hold values from -6 to 6
- gate_c: bfloat16 [2048, 1024], P('sp', 'tp'), may hold values from -6 to 6
- values_in: bfloat16 [2048, 1024], P('sp', 'tp'), may hold values from -6 to 6
- conv_w: bfloat16 [3, 1024], P(None, 'tp'), may hold values from -3.5 to 3.5
- documents: int32 [2048], P('sp'), may hold values from 0 to 2, never falling along the last dimension, each value on 1 to 1024 neighbouring positions
- w_out: bfloat16 [1024, 2048], replicated, may hold values from -0.1875 to 0.1875
- resid: bfloat16 [2048, 2048], P(('sp', 'tp')), may hold values from -6 to 6
- norm_gain: bfloat16 [2048], replicated, may hold values from 0.099609375 to 1.8984375
- route_ids: int32 [2048, 2], P(('sp', 'tp')), may hold values from 0 to 3, all different within a row; in each aligned block of 64 rows (0 to 63, 64 to 127, ...) at most 64 rows name the same one
- route_weight: float32 [2048, 2], P(('sp', 'tp')), may hold values from 0.2 to 1
- w_gate: bfloat16 [4, 2048, 7168], P('sp', None, 'tp'), may hold values from -0.125 to 0.125
- w_up: bfloat16 [4, 2048, 7168], P('sp', None, 'tp'), may hold values from -0.125 to 0.125
- w_down: bfloat16 [4, 7168, 2048], P('sp', 'tp'), may hold values from -0.0625 to 0.0625
Outputs:
- layer_out: bfloat16 [2048, 2048], P(('sp', 'tp'))
Inputs may be any that keep to these rules, and one draw needn't show every extreme that they name: `route_ids`: each token names two different experts; in the rows of one device no expert is named by more than 64 rows, a bound that some block reaches. `documents`: document numbers never fall along the positions; a document has at most 2048 // 2 positions.
All inputs are finite; a program needn't handle non-finite values.
Results may differ from a plain program's by a relative error of at most 0.018.
Values may be sent and summed in bfloat16 or wider, within the bound.
A program may use at most 128 MiB of HBM per device.

v0:
```python
import functools

import jax
import jax.numpy as jnp
from jax import lax
from jax.experimental import pallas as pl
from jax.experimental.pallas import tpu as pltpu
from jax.sharding import PartitionSpec as P

MESH = pl.DeviceIdType.MESH
LANES = 128


def moe_kernel(
    gb, gc, vals, taps, docs, resid, gain, ids, route, wo_hbm, wg_hbm, wu_hbm, wd_hbm, out_ref,
    x_ref, hid, tok, mixed, pad, dpad, hc, hv, hd, wo,
    s_a, r_a, s_h, r_h3,
    xbuf, pbuf, dbuf, r1, r2, rz, wg, wu, wd,
    w_sem, own_sem,
    s_z, r_z, s_1, s_2, r_h, s_p, r_p,
    s_d, r_d, s_r1, r_r1, s_r2, r_r2, s_rz, r_rz,
):
    nz = lax.axis_size("tp") // 2
    pairs = nz // 2
    width = out_ref.shape[1]
    half = width // 2
    rows = out_ref.shape[0]
    sp, tp = lax.axis_index("sp"), lax.axis_index("tp")
    y, x = sp // 2, sp % 2
    z, c = tp // 2, tp % 2
    xn, yn, dg = y * 2 + 1 - x, (1 - y) * 2 + x, (1 - y) * 2 + 1 - x
    other = (sp, z * 2 + 1 - c)
    n_sp, n_tp = lax.axis_size("sp"), lax.axis_size("tp")
    following, previous = (lax.rem(sp + 1, n_sp), tp), (lax.rem(sp + n_sp - 1, n_sp), tp)
    seq = gb.shape[0]
    halo = hc.shape[0]
    to_x, to_y = (xn, tp), (yn, tp)

    def pair_of(q):
        return (z // 2 + q) % pairs

    def zz(k):
        return 2 * pair_of(k // 2) + (z + k) % 2

    def lanes(h):
        return pl.ds(0, half) if h == 0 else pl.ds(half, xbuf.shape[3] - half)

    def rc(src, dst, ss, rs, dev):
        return pltpu.make_async_remote_copy(
            src_ref=src, dst_ref=dst, send_sem=ss, recv_sem=rs,
            device_id=dev, device_id_type=MESH,
        )

    def halo_copies():
        pairs3 = ((gc.at[pl.ds(seq - halo, halo)], hc), (vals.at[pl.ds(seq - halo, halo)], hv),
                  (docs.at[pl.ds(seq - 8, 8)], hd))
        return [rc(a, b, s_h.at[n], r_h3.at[n], following) for n, (a, b) in enumerate(pairs3)]

    def channels(j):
        return pl.ds(pl.multiple_of(j * gb.shape[1], gb.shape[1]), gb.shape[1])

    def swap(d):
        j = lax.rem(tp + d, n_tp)
        at = mixed.at[pl.ds(pl.multiple_of(j * rows, rows), rows)]
        return rc(at, tok.at[:, channels(tp)], s_a.at[d], r_a.at[tp], (sp, j))

    def swapped(d):
        j = lax.rem(tp + d, n_tp)
        at = mixed.at[pl.ds(pl.multiple_of(j * rows, rows), rows)]
        return rc(at, tok.at[:, channels(j)], s_a.at[d], r_a.at[j], (sp, j))

    def mix():
        f32 = jnp.float32
        product = gc[...].astype(f32) * vals[...].astype(f32)
        pad[pl.ds(8, seq)] = product
        dpad[pl.ds(8, seq)] = docs[...]
        for copy in halo_copies():
            copy.wait_recv()
        pad[pl.ds(0, 8)] = (hc[...].astype(f32) * hv[...].astype(f32))[halo - 8 :]
        dpad[pl.ds(0, 8)] = jnp.where(sp == 0, -1, hd[...])
        near = (dpad[pl.ds(7, seq)] == docs[...]).astype(f32)
        far = (dpad[pl.ds(6, seq)] == docs[...]).astype(f32)
        tap = taps[...].astype(f32)
        convolved = (
            tap[2:3] * product
            + tap[1:2] * pad[pl.ds(7, seq)] * near
            + tap[0:1] * pad[pl.ds(6, seq)] * far
        )
        mixed[...] = (gb[...].astype(f32) * convolved).astype(mixed.dtype)
        for d in range(1, n_tp):
            swap(d).start()
        tok[:, channels(tp)] = mixed[pl.ds(pl.multiple_of(tp * rows, rows), rows)]
        lane = lax.broadcasted_iota(jnp.int32, (rows, LANES), 1)
        named = lane % n_sp
        part = lane // n_sp
        share = jnp.where(ids[:, 0:1] == named, route[:, 0:1], 0.0) + jnp.where(
            ids[:, 1:2] == named, route[:, 1:2], 0.0
        )
        high = share.astype(jnp.bfloat16).astype(f32)
        middle = (share - high).astype(jnp.bfloat16).astype(f32)
        low = share - high - middle
        terms = jnp.where(part == 0, high, jnp.where(part == 1, middle, jnp.where(part == 2, low, 0.0)))
        x_ref[:, pl.ds(width, LANES)] = terms.astype(x_ref.dtype)
        wo_copy.wait()
        for d in range(1, n_tp):
            swapped(d).wait_recv()
        projected = jnp.dot(tok[...], wo[...], preferred_element_type=f32)
        hidden = (resid[...].astype(f32) + projected).astype(hid.dtype)
        hid[...] = hidden
        state = hidden.astype(f32)
        mean = jnp.mean(state * state, axis=-1, keepdims=True)
        x_ref[:, pl.ds(0, width)] = (
            state * lax.rsqrt(mean + 1e-06) * gain[...].astype(f32)
        ).astype(x_ref.dtype)

    def z_send(k):
        return rc(x_ref, xbuf.at[sp * nz + z, c], s_z.at[k], r_z.at[z], (sp, zz(k) * 2 + c))

    def z_recv(k):
        return rc(x_ref, xbuf.at[sp * nz + zz(k), c], s_z.at[k], r_z.at[zz(k)], (sp, zz(k) * 2 + c))

    def piece(h, col, k, ss, dev):
        at = xbuf.at[col * nz + zz(k), c, :, lanes(h)]
        return rc(at, at, ss, r_h.at[h, col * nz + zz(k)], dev)

    def first(h, k):
        return piece(h, sp, k, s_1.at[h, k], to_y if h == 0 else to_x)

    def second(h, k):
        return piece(h, sp, k, s_2.at[h, 0, k], to_x if h == 0 else to_y)

    def third(h, k):
        return piece(h, yn if h == 0 else xn, k, s_2.at[h, 1, k], to_x if h == 0 else to_y)

    def arrived(h, col, k):
        piece(h, col, k, s_1.at[h, k], other).wait_recv()

    def to_other(col, k):
        i = col * nz + zz(k)
        return rc(xbuf.at[i, c], xbuf.at[i, c], s_p.at[i], r_p.at[i], other)

    def from_other(i):
        rc(xbuf.at[i, 1 - c], xbuf.at[i, 1 - c], s_p.at[i], r_p.at[i], other).wait_recv()

    def spread(k):
        for h in (1, 0):
            first(h, k).start()
        for h in (0, 1):
            second(h, k).start()
        to_other(sp, k).start()

    def take_z(k):
        z_recv(k).wait_recv()
        spread(k)

    def relay(q):
        for k in (2 * q, 2 * q + 1):
            arrived(0, yn, k)
            third(0, k).start()
            arrived(1, xn, k)
            third(1, k).start()

    def sides(q):
        for k in (2 * q, 2 * q + 1):
            arrived(0, xn, k)
            to_other(xn, k).start()
            arrived(1, yn, k)
            to_other(yn, k).start()

    def corner(q):
        for k in (2 * q, 2 * q + 1):
            arrived(0, dg, k)
            arrived(1, dg, k)
            to_other(dg, k).start()

    def d_copy(col, p, mine):
        i = pl.ds(col * nz + 2 * p, 2)
        at = pbuf.at[i, 1 - c]
        return rc(at, dbuf.at[i], s_d.at[col * pairs + p], r_d.at[col * pairs + p], other)

    def cols(h):
        return pl.ds(h * half, half)

    def r1_copy(h, o, p):
        col = dg if o else (xn if h == 0 else yn)
        at = pbuf.at[pl.ds(col * nz + 2 * p, 2), c, :, cols(h)]
        return rc(at, r1.at[h, o, pl.ds(2 * p, 2)], s_r1.at[h, o, p], r_r1.at[h, o, p], to_x if h == 0 else to_y)

    def r2_copy(h, p):
        col = yn if h == 0 else xn
        at = pbuf.at[pl.ds(col * nz + 2 * p, 2), c, :, cols(h)]
        return rc(at, r2.at[h, pl.ds(2 * p, 2)], s_r2.at[h, p], r_r2.at[h, p], to_y if h == 0 else to_x)

    def rz_copy(k):
        return rc(pbuf.at[sp * nz + zz(k), c], rz.at[z], s_rz.at[k], r_rz.at[z], (sp, zz(k) * 2 + c))

    def rz_recv(k):
        return rc(pbuf.at[sp * nz + zz(k), c], rz.at[zz(k)], s_rz.at[k], r_rz.at[zz(k)], (sp, zz(k) * 2 + c))

    f32 = jnp.float32

    def merge(fy, fx, p):
        col = (y + fy - 2 * y * fy) * 2 + x + fx - 2 * x * fx
        d_copy(col, p, False).wait_recv()
        i = pl.ds(col * nz + 2 * p, 2)
        pbuf[i, c] = (pbuf[i, c].astype(f32) + dbuf[i].astype(f32)).astype(pbuf.dtype)

    def send_sum(g, p):
        @pl.when(g == 1)
        def _():
            r1_copy(0, 0, p).start()

        @pl.when(g == 2)
        def _():
            r1_copy(1, 0, p).start()

        @pl.when(g == 3)
        def _():
            r1_copy(0, 1, p).start()
            r1_copy(1, 1, p).start()

    def stage2(q):
        p = pair_of(q)
        for h in (0, 1):
            r1_copy(h, 1, p).wait_recv()
            col = yn if h == 0 else xn
            i = pl.ds(col * nz + 2 * p, 2)
            pbuf[i, c, :, cols(h)] = (
                pbuf[i, c, :, cols(h)].astype(f32) + r1[h, 1, pl.ds(2 * p, 2)].astype(f32)
            ).astype(pbuf.dtype)
            r2_copy(h, p).start()

    def stage3(q):
        p = pair_of(q)
        i = pl.ds(sp * nz + 2 * p, 2)
        j = pl.ds(2 * p, 2)
        for h in (0, 1):
            r1_copy(h, 0, p).wait_recv()
            r2_copy(h, p).wait_recv()
            pbuf[i, c, :, cols(h)] = (
                pbuf[i, c, :, cols(h)].astype(f32)
                + r1[h, 0, j].astype(f32)
                + r2[h, j].astype(f32)
            ).astype(pbuf.dtype)
        for k in (2 * q, 2 * q + 1):
            if k > 0:
                rz_copy(k).start()

    weights = [
        pltpu.make_async_copy(a, b, w_sem.at[n])
        for n, (a, b) in enumerate(((wg_hbm, wg), (wu_hbm, wu), (wd_hbm, wd)))
    ]
    own = pltpu.make_async_copy(x_ref, xbuf.at[sp * nz + z, c], own_sem)
    wo_copy = pltpu.make_async_copy(wo_hbm, wo, w_sem.at[3])
    wo_copy.start()
    for w in weights:
        w.start()
    barrier = pltpu.get_barrier_semaphore()
    peers = [to_x, to_y, following, previous] + [(sp, lax.rem(tp + d, n_tp)) for d in range(1, n_tp)]
    for peer in peers:
        pl.semaphore_signal(barrier, inc=1, device_id=peer, device_id_type=MESH)
    pl.semaphore_wait(barrier, len(peers))
    for copy in halo_copies():
        copy.start()
    mix()
    own.start()
    for k in range(1, nz):
        z_send(k).start()
    own.wait()
    spread(0)
    take_z(1)
    for w in weights:
        w.wait()

    experts_lanes = lax.axis_size("sp")
    lane = lax.broadcasted_iota(jnp.int32, (1, LANES), 1)
    mine = ((lane % experts_lanes == sp) & (lane < 3 * experts_lanes)).astype(f32)

    before = {1: [lambda: relay(0), lambda: sides(0)]}
    for q in range(1, pairs):
        base = 4 * (q - 1)
        before.setdefault(base + 2, []).append(functools.partial(take_z, 2 * q))
        before.setdefault(base + 3, []).append(functools.partial(take_z, 2 * q + 1))
        before.setdefault(4 * q + 1, []).append(functools.partial(relay, q))
        before.setdefault(4 * q + 1, []).append(functools.partial(sides, q))
    for q in range(pairs):
        before.setdefault(4 * q + 3, []).append(functools.partial(corner, q))
    after = {}
    for q in range(pairs - 1):
        after.setdefault(4 * q + 6, []).append(functools.partial(stage2, q))

    @pl.loop(0, 4 * pairs)
    def _(s):
        for at, works in before.items():
            @pl.when(s == at)
            def _():
                for work in works:
                    work()

        g = s % 4
        fy, fx = g // 2, g % 2
        p = pair_of(s // 4)
        col = (y + fy - 2 * y * fy) * 2 + x + fx - 2 * x * fx
        i = col * nz + 2 * p
        for b in (0, 1):
            from_other(i + b)
        held = xbuf[pl.ds(i, 2)].reshape(4 * rows, xbuf.shape[3])
        scale = jnp.sum(held[:, width:].astype(f32) * mine, axis=1, keepdims=True)
        held = held[:, :width]
        gate = jnp.dot(held, wg[...], preferred_element_type=f32)
        up = jnp.dot(held, wu[...], preferred_element_type=f32)
        act = (jax.nn.silu(gate) * up * scale).astype(jnp.bfloat16)
        part = jnp.dot(act, wd[...], preferred_element_type=f32)
        pbuf[pl.ds(i, 2)] = part.astype(pbuf.dtype).reshape(2, 2, rows, width)
        d_copy(col, p, True).start()

        @pl.when(s > 0)
        def _():
            t = s - 1
            gt = t % 4
            pt = pair_of(t // 4)
            merge(gt // 2, gt % 2, pt)
            send_sum(gt, pt)

        for at, works in after.items():
            @pl.when(s == at)
            def _():
                for work in works:
                    work()

    last = pair_of(pairs - 1)
    merge(1, 1, last)
    send_sum(3, last)
    for q in range(pairs - 1):
        stage3(q)
    stage2(pairs - 1)
    stage3(pairs - 1)
    total = pbuf[sp * nz + z, c].astype(f32)
    for k in range(1, nz):
        rz_recv(k).wait_recv()
        total = total + rz[zz(k)].astype(f32)
    out_ref[...] = (hid[...].astype(f32) + total).astype(out_ref.dtype)

    for copy in halo_copies():
        copy.wait_send()
    for d in range(1, n_tp):
        swap(d).wait_send()
    for k in range(1, nz):
        z_send(k).wait_send()
        rz_copy(k).wait_send()
    for k in range(nz):
        for h in (0, 1):
            first(h, k).wait_send()
            second(h, k).wait_send()
            third(h, k).wait_send()
        for col in (sp, xn, yn, dg):
            to_other(col, k).wait_send()
    for q in range(pairs):
        p = pair_of(q)
        for col in (sp, xn, yn, dg):
            d_copy(col, p, True).wait_send()
        for h in (0, 1):
            for o in (0, 1):
                r1_copy(h, o, p).wait_send()
            r2_copy(h, p).wait_send()


def layer(gate_b, gate_c, values_in, conv_w, docs, resid, gain, ids, route, w_out, w_gate, w_up, w_down):
    rows, width = resid.shape
    wide = width + LANES
    seq, held = gate_b.shape
    n_tp = lax.axis_size("tp")
    n_sp = lax.axis_size("sp")
    nz = lax.axis_size("tp") // 2
    pairs = nz // 2
    half = width // 2
    bf = jnp.bfloat16
    dma = pltpu.SemaphoreType.DMA
    hbm = pl.BlockSpec(memory_space=pl.ANY)
    vmem = pl.BlockSpec(memory_space=pltpu.VMEM)
    return pl.pallas_call(
        moe_kernel,
        out_shape=jax.ShapeDtypeStruct((rows, width), bf),
        in_specs=[vmem] * 9 + [hbm] * 4,
        out_specs=vmem,
        scratch_shapes=[
            pltpu.VMEM((rows, wide), bf),
            pltpu.VMEM((rows, width), bf),
            pltpu.VMEM((rows, n_tp * held), bf),
            pltpu.VMEM((seq, held), bf),
            pltpu.VMEM((seq + 8, held), jnp.float32),
            pltpu.VMEM((seq + 8, held), jnp.int32),
            pltpu.VMEM((16, held), bf),
            pltpu.VMEM((16, held), bf),
            pltpu.VMEM((8, held), jnp.int32),
            pltpu.VMEM(w_out.shape, bf),
            dma((n_tp,)), dma((n_tp,)), dma((3,)), dma((3,)),
            pltpu.VMEM((n_sp * nz, 2, rows, wide), bf),
            pltpu.VMEM((n_sp * nz, 2, rows, width), bf),
            pltpu.VMEM((n_sp * nz, rows, width), bf),
            pltpu.VMEM((2, 2, nz, rows, half), bf),
            pltpu.VMEM((2, nz, rows, half), bf),
            pltpu.VMEM((nz, rows, width), bf),
            pltpu.VMEM(w_gate.shape, bf),
            pltpu.VMEM(w_up.shape, bf),
            pltpu.VMEM(w_down.shape, bf),
            dma((4,)), dma,
            dma((nz,)), dma((nz,)),
            dma((2, nz)), dma((2, 2, nz)), dma((2, n_sp * nz)),
            dma((n_sp * nz,)), dma((n_sp * nz,)),
            dma((n_sp * pairs,)), dma((n_sp * pairs,)),
            dma((2, 2, pairs)), dma((2, 2, pairs)),
            dma((2, pairs)), dma((2, pairs)),
            dma((nz,)), dma((nz,)),
        ],
        compiler_params=pltpu.CompilerParams(
            collective_id=0, has_side_effects=True, vmem_limit_bytes=64000000
        ),
    )(gate_b, gate_c, values_in, conv_w, docs, resid, gain, ids, route, w_out, w_gate, w_up, w_down)


def passed_along(block, axis, distance):
    devices = range(lax.axis_size(axis))
    route = [(i - distance, i) for i in devices if i - distance in devices]
    return lax.ppermute(block, axis, route)


def local(
    gate_b,
    gate_c,
    values_in,
    conv_w,
    documents,
    w_out,
    resid,
    norm_gain,
    route_ids,
    route_weight,
    w_gate,
    w_up,
    w_down,
):
    seq_rows = gate_b.shape[0]
    local_rows = resid.shape[0]
    model_width = resid.shape[1]
    experts = lax.axis_size("sp") * w_gate.shape[0]
    capacity = 4 * local_rows // experts
    if lax.axis_size("sp") == 4 and w_gate.shape[0] == 1 and capacity >= local_rows:
        docs = jnp.broadcast_to(documents[:, None], gate_b.shape)
        return layer(
            gate_b, gate_c, values_in, conv_w, docs, resid, norm_gain[None, :], route_ids,
            route_weight, w_out, w_gate[0], w_up[0], w_down[0],
        )
    last_rows = jnp.stack([gate_c[seq_rows - 2 :], values_in[seq_rows - 2 :]])
    before, before_docs = passed_along((last_rows, documents[seq_rows - 2 :]), "sp", 1)
    products = jnp.concatenate(
        [
            before[0].astype(jnp.float32) * before[1].astype(jnp.float32),
            gate_c.astype(jnp.float32) * values_in.astype(jnp.float32),
        ],
        axis=0,
    )
    docs_all = jnp.concatenate([before_docs, documents], axis=0)
    kernel_taps = conv_w.astype(jnp.float32)
    near_mask = (docs_all[1:-1] == documents).astype(jnp.float32)[:, None]
    far_mask = (docs_all[:-2] == documents).astype(jnp.float32)[:, None]
    convolved = (
        kernel_taps[2] * products[2:]
        + kernel_taps[1] * products[1:-1] * near_mask
        + kernel_taps[0] * products[:-2] * far_mask
    )
    mixed_rows = (gate_b.astype(jnp.float32) * convolved).astype(jnp.bfloat16)
    token_rows = lax.all_to_all(mixed_rows, "tp", split_axis=0, concat_axis=1, tiled=True)
    projected = jnp.dot(token_rows, w_out, preferred_element_type=jnp.float32)
    hidden_state = (resid.astype(jnp.float32) + projected).astype(jnp.bfloat16)
    state_wide = hidden_state.astype(jnp.float32)
    normed = (
        state_wide
        * lax.rsqrt(jnp.mean(state_wide * state_wide, axis=-1, keepdims=True) + 1e-06)
        * norm_gain.astype(jnp.float32)
    ).astype(jnp.bfloat16)
    experts = lax.axis_size("sp") * w_gate.shape[0]
    capacity = 4 * local_rows // experts
    flat_ids = route_ids.reshape(-1)
    one_hot = (flat_ids[:, None] == jnp.arange(experts, dtype=jnp.int32)[None, :]).astype(jnp.int32)
    rank_in = jnp.sum((jnp.cumsum(one_hot, axis=0) - one_hot) * one_hot, axis=1)
    slot_index = flat_ids * capacity + rank_in
    placement = (
        slot_index[:, None] == jnp.arange(experts * capacity, dtype=jnp.int32)[None, :]
    ).astype(jnp.bfloat16)
    repeated = jnp.repeat(normed, 2, axis=0)
    dispatch = jnp.einsum(
        "js,jd->sd", placement, repeated, preferred_element_type=jnp.float32
    ).astype(jnp.bfloat16)
    dispatch = dispatch.reshape(experts, capacity, model_width)
    gathered_piece = lax.all_gather(
        lax.all_to_all(dispatch, "sp", split_axis=0, concat_axis=0, tiled=True),
        "tp",
        axis=0,
        tiled=True,
    )
    flat_rows = gathered_piece.reshape(-1, model_width)
    gate_part = jnp.dot(flat_rows, w_gate[0], preferred_element_type=jnp.float32)
    up_part = jnp.dot(flat_rows, w_up[0], preferred_element_type=jnp.float32)
    activated = (jax.nn.silu(gate_part) * up_part).astype(jnp.bfloat16)
    partial_value = jnp.dot(activated, w_down[0], preferred_element_type=jnp.float32)
    partial_value = partial_value.reshape(
        gathered_piece.shape[0], gathered_piece.shape[1], model_width
    )
    summed = lax.psum_scatter(
        partial_value.astype(jnp.bfloat16), "tp", scatter_dimension=0, tiled=True
    )
    returned = lax.all_to_all(summed, "sp", split_axis=0, concat_axis=0, tiled=True)
    picked = jnp.take(
        returned.reshape(experts * capacity, model_width), slot_index, axis=0
    ).reshape(local_rows, 2, model_width)
    combined = jnp.sum(route_weight[:, :, None] * picked.astype(jnp.float32), axis=1)
    return (hidden_state.astype(jnp.float32) + combined).astype(jnp.bfloat16)


def solution(mesh):
    return jax.shard_map(
        local,
        mesh=mesh,
        in_specs=(
            P("sp", "tp"),
            P("sp", "tp"),
            P("sp", "tp"),
            P(None, "tp"),
            P("sp"),
            P(),
            P(("sp", "tp"), None),
            P(),
            P(("sp", "tp"), None),
            P(("sp", "tp"), None),
            P("sp", None, "tp"),
            P("sp", None, "tp"),
            P("sp", "tp", None),
        ),
        out_specs=P(("sp", "tp"), None),
        check_vma=False,
    )
```

profile of v0, /device:TPU:10, one launch (start us, length us, event | category | flops | bytes accessed | tf_op | source)
XLA Modules:
  0.0 124.4 jit_solution(13979715403656771120)
XLA Ops:
  0.0 1.3 %broadcast_in_dim.10.gain = bf16[1,2048]{1,0:T(2,128)(2,1)} reshape(bf16[2048]{0:T(1024)(128)(2,1)} %param.20) | data formatting | bytes 8192 | tf_op jit(solution)/shard_map/broadcast_in_dim | solution.py:451
  1.3 1.4 %copy.14.ids = s32[64,2]{1,0:T(8,128)} copy(s32[64,2]{0,1:T(2,128)} %param.21) | data formatting | bytes 1024 | tf_op args[8]
  2.6 1.4 %copy.15.route = f32[64,2]{1,0:T(8,128)} copy(f32[64,2]{0,1:T(2,128)} %param.22) | data formatting | bytes 1024 | tf_op args[9]
  4.0 1.5 %broadcast_in_dim.4.docs = s32[512,128]{1,0:T(8,128)} broadcast(s32[512]{0:T(512)} %param.17), dimensions={0} | broadcast | bytes 264192 | tf_op jit(solution)/shard_map/broadcast_in_dim | solution.py:449
  5.5 117.1 %shard_map.127 = bf16[64,2048]{1,0:T(8,128)(2,1)} custom-call(bf16[512,128]{1,0:T(8,128)(2,1)} %gb.1, bf16[512,128]{1,0:T(8,128)(2,1)} %gc.1, bf16[512,128]{1,0:T(8,128)(2,1)} %vals.1, bf16[3,128]{1,0:T(4,128)(2,1)} %taps.1, s32[512,128]{1,0:T(8,128)} %broadcast_in_dim.4.docs, bf16[64,2048]{1,0:T(8,128)(2,1)} %resid.1, ...), custom_call_target="tpu_custom_call" | custom-call | tf_op jit(solution)/shard_map/pallas_call | solution.py:381
  122.7 1.7 %copy.17 = bf16[64,2048]{1,0:T(8,128)(2,1)} copy(bf16[64,2048]{1,0:T(8,128)(2,1)} %shard_map.127) | data formatting | bytes 524288
where the time goes:
time: 125 us; the launch traced here: 124 us
  Pallas kernels  117 us (94%)
  local copies, waits for them, and re-layouts  7.2 us (6%)
    pallas_call x1, Pallas kernels, layer(): pl.pallas_call(moe_kernel, out_shape=jax.ShapeDtypeStruct((rows, width),...  117 us
    unnamed x3, local copies, waits for them, and re-layouts  4.4 us

commit v1 on v0

v1 whole, which is shorter than its diff:
```python
import functools

import jax
import jax.numpy as jnp
from jax import lax
from jax.experimental import pallas as pl
from jax.experimental.pallas import tpu as pltpu
from jax.sharding import PartitionSpec as P

MESH = pl.DeviceIdType.MESH
LANES = 128


def moe_kernel(
    gb_hbm, gc_hbm, vals_hbm, taps_hbm, docs_hbm, resid_hbm, gain_hbm, ids_hbm, route_hbm,
    wo_hbm, wg_hbm, wu_hbm, wd_hbm, out_ref,
    gb, gc, vals, taps, docs, resid, gain, ids, route,
    hid, tok, mixed, pad, dpad, mat, hc, hv, hd, wo,
    xbuf, pbuf, dbuf, r1, r2, rz, wg, wu, wd,
    in_sem, w_sem,
    s_a, r_a, s_b, s_h, r_h3,
    s_z, r_z, s_1, s_2, r_h, s_p, r_p,
    s_d, r_d, s_r1, r_r1, s_r2, r_r2, s_rz, r_rz,
):
    f32 = jnp.float32
    n_sp, n_tp = lax.axis_size("sp"), lax.axis_size("tp")
    nz = n_tp // 2
    width = out_ref.shape[1]
    half = width // 2
    rows = out_ref.shape[0]
    seq = gb.shape[0]
    halo = hc.shape[0]
    sp, tp = lax.axis_index("sp"), lax.axis_index("tp")
    y, x = sp // 2, sp % 2
    z, c = tp // 2, tp % 2
    xn, yn, dg = y * 2 + 1 - x, (1 - y) * 2 + x, (1 - y) * 2 + 1 - x
    columns = (sp, xn, yn, dg)
    OWN, XN, YN, DG = range(4)
    other = (sp, z * 2 + 1 - c)
    following, previous = (lax.rem(sp + 1, n_sp), tp), (lax.rem(sp + n_sp - 1, n_sp), tp)
    to_x, to_y = (xn, tp), (yn, tp)

    def zz(k):
        if k < 2:
            return 2 * (z // 2) + (z + k) % 2
        return k + (z // 2) * (nz - 1 - 2 * k)

    def slot(k, rel):
        return zz(k) * n_sp + columns[rel]

    def lanes(h):
        return pl.ds(0, half) if h == 0 else pl.ds(half, xbuf.shape[3] - half)

    def cols(h):
        return pl.ds(h * half, half)

    def rc(src, dst, ss, rs, dev):
        return pltpu.make_async_remote_copy(
            src_ref=src, dst_ref=dst, send_sem=ss, recv_sem=rs,
            device_id=dev, device_id_type=MESH,
        )


    def halo_copies():
        pairs = (
            (gc.at[pl.ds(seq - halo, halo)], hc),
            (vals.at[pl.ds(seq - halo, halo)], hv),
            (docs, hd),
        )
        return [rc(a, b, s_h.at[n], r_h3.at[n], following) for n, (a, b) in enumerate(pairs)]

    def channels(j):
        return pl.ds(pl.multiple_of(j * gb.shape[1], gb.shape[1]), gb.shape[1])

    def token_rows(j):
        return mixed.at[pl.ds(pl.multiple_of(j * rows, rows), rows)]

    def swap(d):
        j = lax.rem(tp + d, n_tp)
        return rc(token_rows(j), tok.at[:, channels(tp)], s_a.at[d], r_a.at[tp], (sp, j))

    def swapped(d):
        j = lax.rem(tp + d, n_tp)
        return rc(token_rows(j), tok.at[:, channels(j)], s_a.at[d], r_a.at[j], (sp, j))

    def swap_first():
        return rc(token_rows(0), tok.at[:, channels(tp)], s_b, r_a.at[tp], (sp, 0))

    def convolve(first, count):
        own = pl.ds(first, count)
        now = dpad[pl.ds(first + 8, count)]
        near = (dpad[pl.ds(first + 7, count)] == now).astype(f32)
        far = (dpad[pl.ds(first + 6, count)] == now).astype(f32)
        tap = taps[...].astype(f32)
        convolved = (
            tap[2:3] * pad[pl.ds(first + 8, count)]
            + tap[1:2] * pad[pl.ds(first + 7, count)] * near
            + tap[0:1] * pad[pl.ds(first + 6, count)] * far
        )
        mixed[own] = (gb[own].astype(f32) * convolved).astype(mixed.dtype)

    def mix():
        mat[...] = jnp.zeros_like(mat)
        doc_rows = docs.shape[0]
        mat[pl.ds(0, doc_rows)] = docs[...].astype(f32)
        mat[pl.ds(doc_rows, 2), pl.ds(0, rows)] = ids[...].astype(f32)
        mat[pl.ds(doc_rows + 2, 2), pl.ds(0, rows)] = route[...]
        turned = mat[...].T
        for n in range(doc_rows):
            dpad[pl.ds(8 + n * LANES, LANES)] = jnp.broadcast_to(
                turned[:, n : n + 1], (LANES, dpad.shape[1])
            )
        pad[pl.ds(8, seq)] = gc[...].astype(f32) * vals[...].astype(f32)
        pad[pl.ds(0, 8)] = jnp.zeros((8, pad.shape[1]), f32)
        dpad[pl.ds(0, 8)] = jnp.full((8, dpad.shape[1]), -1.0, f32)
        convolve(0, seq)
        for d in range(1, n_tp):
            @pl.when(lax.rem(tp + d, n_tp) != 0)
            def _():
                swap(d).start()

        lane = lax.broadcasted_iota(jnp.int32, (rows, LANES), 1)
        named = (lane % n_sp).astype(f32)
        part = lane // n_sp
        side = turned[:rows]
        at = doc_rows
        share = jnp.where(side[:, at : at + 1] == named, side[:, at + 2 : at + 3], 0.0) + jnp.where(
            side[:, at + 1 : at + 2] == named, side[:, at + 3 : at + 4], 0.0
        )
        high = share.astype(jnp.bfloat16).astype(f32)
        middle = (share - high).astype(jnp.bfloat16).astype(f32)
        low = share - high - middle
        terms = jnp.where(part == 0, high, jnp.where(part == 1, middle, jnp.where(part == 2, low, 0.0)))
        mine = z * n_sp + sp
        xbuf[c, mine, :, pl.ds(width, LANES)] = terms.astype(xbuf.dtype)

        for copy in halo_copies():
            copy.wait_recv()
        pad[pl.ds(0, 8)] = (hc[...].astype(f32) * hv[...].astype(f32))[halo - 8 :]
        last = hd[pl.ds(doc_rows - 1, 1)].astype(f32)
        last = jnp.where(sp == 0, -1.0, last)
        for n in (1, 2):
            dpad[pl.ds(8 - n, 1)] = jnp.broadcast_to(
                last[:, LANES - n : LANES - n + 1], (1, dpad.shape[1])
            )
        convolve(0, 16)

        @pl.when(tp != 0)
        def _():
            swap_first().start()

        tok[:, channels(tp)] = mixed[pl.ds(pl.multiple_of(tp * rows, rows), rows)]
        in_copies[5].wait()
        in_copies[6].wait()
        wo_copy.wait()
        for d in range(1, n_tp):
            swapped(d).wait_recv()
        projected = jnp.dot(tok[...], wo[...], preferred_element_type=f32)
        hidden = (resid[...].astype(f32) + projected).astype(hid.dtype)
        hid[...] = hidden
        state = hidden.astype(f32)
        scale = lax.rsqrt(jnp.mean(state * state, axis=-1, keepdims=True) + 1e-06)
        for n in range(width // LANES):
            at = slice(n * LANES, (n + 1) * LANES)
            xbuf[c, mine, :, pl.ds(n * LANES, LANES)] = (
                state[:, at] * scale * gain[n : n + 1].astype(f32)
            ).astype(xbuf.dtype)


    def z_send(k):
        at = xbuf.at[c, z * n_sp + sp]
        return rc(at, at, s_z.at[k], r_z.at[z], (sp, zz(k) * 2 + c))

    def z_recv(k):
        at = xbuf.at[c, slot(k, OWN)]
        return rc(at, at, s_z.at[k], r_z.at[zz(k)], (sp, zz(k) * 2 + c))

    def piece(h, rel, k, ss, there, dev):
        at = xbuf.at[c, slot(k, rel), :, lanes(h)]
        return rc(at, at, ss, r_h.at[h, there, k], dev)

    def first(h, k):
        return piece(h, OWN, k, s_1.at[h, k], YN if h == 0 else XN, to_y if h == 0 else to_x)

    def second(h, k):
        return piece(h, OWN, k, s_2.at[h, 0, k], XN if h == 0 else YN, to_x if h == 0 else to_y)

    def third(h, k):
        return piece(h, YN if h == 0 else XN, k, s_2.at[h, 1, k], DG, to_x if h == 0 else to_y)

    def arrived(h, rel, k):
        piece(h, rel, k, s_1.at[h, k], rel, other).wait_recv()

    def to_other(rel, k):
        at = xbuf.at[c, slot(k, rel)]
        return rc(at, at, s_p.at[k * n_sp + rel], r_p.at[k * n_sp + rel], other)

    def spread(k):
        for h in (1, 0):
            first(h, k).start()
        for h in (0, 1):
            second(h, k).start()
        to_other(OWN, k).start()

    def take(k):
        z_recv(k).wait_recv()
        spread(k)

    def relay(k):
        arrived(0, YN, k)
        third(0, k).start()
        arrived(1, XN, k)
        third(1, k).start()

    def sides(k):
        arrived(0, XN, k)
        to_other(XN, k).start()
        arrived(1, YN, k)
        to_other(YN, k).start()

    def corner(k):
        arrived(0, DG, k)
        arrived(1, DG, k)
        to_other(DG, k).start()


    def group(k):
        return pl.ds(zz(k) * n_sp, n_sp)

    def d_copy(k):
        return rc(pbuf.at[1 - c, group(k)], dbuf.at[group(k)], s_d.at[k], r_d.at[k], other)

    def merge(k):
        d_copy(k).wait_recv()
        i = group(k)
        pbuf[c, i] = (pbuf[c, i].astype(f32) + dbuf[i].astype(f32)).astype(pbuf.dtype)

    def r1_copy(h, o, k):
        rel = DG if o else (XN if h == 0 else YN)
        at = pbuf.at[c, slot(k, rel), :, cols(h)]
        return rc(at, r1.at[h, o, k], s_r1.at[h, o, k], r_r1.at[h, o, k], to_x if h == 0 else to_y)

    def r2_copy(h, k):
        at = pbuf.at[c, slot(k, YN if h == 0 else XN), :, cols(h)]
        return rc(at, r2.at[h, k], s_r2.at[h, k], r_r2.at[h, k], to_y if h == 0 else to_x)

    def rz_copy(k):
        at = pbuf.at[c, slot(k, OWN)]
        return rc(at, rz.at[z], s_rz.at[k], r_rz.at[z], (sp, zz(k) * 2 + c))

    def rz_recv(k):
        at = pbuf.at[c, slot(k, OWN)]
        return rc(at, rz.at[zz(k)], s_rz.at[k], r_rz.at[zz(k)], (sp, zz(k) * 2 + c))

    def stage1(k, parts=(1, 0)):
        for o in parts:
            for h in (0, 1):
                r1_copy(h, o, k).start()

    def stage2(k):
        for h in (0, 1):
            r1_copy(h, 1, k).wait_recv()
            i = slot(k, YN if h == 0 else XN)
            pbuf[c, i, :, cols(h)] = (
                pbuf[c, i, :, cols(h)].astype(f32) + r1[h, 1, k].astype(f32)
            ).astype(pbuf.dtype)
            r2_copy(h, k).start()

    def summed(h, k):
        r1_copy(h, 0, k).wait_recv()
        r2_copy(h, k).wait_recv()
        return (
            pbuf[c, slot(k, OWN), :, cols(h)].astype(f32)
            + r1[h, 0, k].astype(f32)
            + r2[h, k].astype(f32)
        )

    def stage3(k):
        for h in (0, 1):
            pbuf[c, slot(k, OWN), :, cols(h)] = summed(h, k).astype(pbuf.dtype)
        rz_copy(k).start()

    barrier = pltpu.get_barrier_semaphore()
    peers = [to_x, to_y, following, previous] + [(sp, lax.rem(tp + d, n_tp)) for d in range(1, n_tp)]
    for peer in peers:
        pl.semaphore_signal(barrier, inc=1, device_id=peer, device_id_type=MESH)
    in_copies = [
        pltpu.make_async_copy(a, b, in_sem.at[n])
        for n, (a, b) in enumerate((
            (gc_hbm, gc), (vals_hbm, vals), (docs_hbm, docs), (taps_hbm, taps), (gb_hbm, gb),
            (resid_hbm, resid), (gain_hbm, gain), (ids_hbm, ids), (route_hbm, route),
        ))
    ]
    weights = [
        pltpu.make_async_copy(a, b, w_sem.at[n])
        for n, (a, b) in enumerate(((wg_hbm, wg), (wu_hbm, wu), (wd_hbm, wd)))
    ]
    wo_copy = pltpu.make_async_copy(wo_hbm, wo, w_sem.at[3])
    for copy in in_copies:
        copy.start()
    wo_copy.start()
    for w in weights:
        w.start()
    for n in (0, 1, 2):
        in_copies[n].wait()
    pl.semaphore_wait(barrier, len(peers))
    for copy in halo_copies():
        copy.start()
    for n in (3, 4, 7, 8):
        in_copies[n].wait()
    mix()
    for h in (1, 0):
        first(h, 0).start()
    for k in range(1, nz):
        z_send(k).start()
    for h in (0, 1):
        second(h, 0).start()
    to_other(OWN, 0).start()
    relay(0)
    take(1)
    sides(0)
    corner(0)
    for w in weights:
        w.wait()

    lane = lax.broadcasted_iota(jnp.int32, (1, LANES), 1)
    chosen = ((lane % n_sp == sp) & (lane < 3 * n_sp)).astype(f32)

    steps = 2 * nz
    before, after = {}, {}

    def put(table, s, work, *args):
        table.setdefault(s, []).append(functools.partial(work, *args))

    end = nz - 1
    for k in range(1, nz):
        put(before, 2 * k - 1, relay, k)
        if k < end:
            put(before, 2 * k, take, k + 1)
        put(before, 2 * k, sides, k)
        put(before, 2 * k, corner, k)
    for k in range(end - 1):
        put(after, 2 * k + 2, merge, k)
        if k > 0:
            put(before, 2 * k + 3, stage1, k)
    put(before, 2 * end, merge, end - 1)
    put(before, 2 * end, stage1, end - 1)
    put(before, 2 * end + 1, stage2, 1)

    @pl.loop(0, steps)
    def _(s):
        for at, works in before.items():
            @pl.when(s == at)
            def _():
                for work in works:
                    work()

        k = s // 2
        shared = (s + k // (nz - 1)) % 2
        core = (c + shared) % 2
        at_z = jnp.where(k < 2, 2 * (z // 2) + (z + k) % 2, k + (z // 2) * (nz - 1 - 2 * k))
        i = pl.ds(at_z * n_sp, n_sp)

        @pl.when(shared == 1)
        def _():
            for rel in range(n_sp):
                at = xbuf.at[1 - c, at_z * n_sp + rel]
                n = k * n_sp + rel
                rc(at, at, s_p.at[n], r_p.at[n], other).wait_recv()

        held = xbuf[core, i].reshape(n_sp * rows, xbuf.shape[3])
        scale = jnp.sum(held[:, width:].astype(f32) * chosen, axis=1, keepdims=True)
        held = held[:, :width]
        gate = jnp.dot(held, wg[...], preferred_element_type=f32)
        up = jnp.dot(held, wu[...], preferred_element_type=f32)
        act = (jax.nn.silu(gate) * up * scale).astype(jnp.bfloat16)
        down = jnp.dot(act, wd[...], preferred_element_type=f32)
        pbuf[core, i] = down.astype(pbuf.dtype).reshape(n_sp, rows, width)

        @pl.when(shared == 1)
        def _():
            rc(pbuf.at[1 - c, i], dbuf.at[i], s_d.at[k], r_d.at[k], other).start()

        for at, works in after.items():
            @pl.when(s == at)
            def _():
                for work in works:
                    work()

    merge(end)
    stage1(end)
    for k in range(2, end):
        stage2(k)
    stage1(0, (1,))
    stage3(1)
    stage2(end)
    stage1(0, (0,))
    for k in range(2, end):
        stage3(k)
    stage3(end)
    stage2(0)
    for h in (0, 1):
        total = summed(h, 0)
        for k in range(1, nz):
            if h == 0:
                rz_recv(k).wait_recv()
            total = total + rz[zz(k), :, cols(h)].astype(f32)
        out_ref[:, cols(h)] = (hid[:, cols(h)].astype(f32) + total).astype(out_ref.dtype)

    for copy in halo_copies():
        copy.wait_send()
    for d in range(1, n_tp):
        @pl.when(lax.rem(tp + d, n_tp) != 0)
        def _():
            swap(d).wait_send()

    @pl.when(tp != 0)
    def _():
        swap_first().wait_send()

    for k in range(1, nz):
        z_send(k).wait_send()
        rz_copy(k).wait_send()
    for k in range(nz):
        for h in (0, 1):
            first(h, k).wait_send()
            second(h, k).wait_send()
            third(h, k).wait_send()
            r1_copy(h, 0, k).wait_send()
            r1_copy(h, 1, k).wait_send()
            r2_copy(h, k).wait_send()
        for rel in range(n_sp):
            to_other(rel, k).wait_send()
    for k in range(nz):
        d_copy(k).wait_send()


def layer(gate_b, gate_c, values_in, conv_w, docs, resid, gain, ids, route, w_out, w_gate, w_up, w_down):
    rows, width = resid.shape
    wide = width + LANES
    seq, held = gate_b.shape
    n_tp = lax.axis_size("tp")
    n_sp = lax.axis_size("sp")
    nz = n_tp // 2
    half = width // 2
    bf = jnp.bfloat16
    f32 = jnp.float32
    dma = pltpu.SemaphoreType.DMA
    hbm = pl.BlockSpec(memory_space=pl.ANY)
    vmem = pl.BlockSpec(memory_space=pltpu.VMEM)
    operands = (gate_b, gate_c, values_in, conv_w, docs, resid, gain, ids, route)
    return pl.pallas_call(
        moe_kernel,
        out_shape=jax.ShapeDtypeStruct((rows, width), bf),
        in_specs=[hbm] * 13,
        out_specs=vmem,
        scratch_shapes=[pltpu.VMEM(a.shape, a.dtype) for a in operands] + [
            pltpu.VMEM((rows, width), bf),
            pltpu.VMEM((rows, n_tp * held), bf),
            pltpu.VMEM((seq, held), bf),
            pltpu.VMEM((seq + 8, held), f32),
            pltpu.VMEM((seq + 8, held), f32),
            pltpu.VMEM((LANES, LANES), f32),
            pltpu.VMEM((16, held), bf),
            pltpu.VMEM((16, held), bf),
            pltpu.VMEM(docs.shape, docs.dtype),
            pltpu.VMEM(w_out.shape, bf),
            pltpu.VMEM((2, n_sp * nz, rows, wide), bf),
            pltpu.VMEM((2, n_sp * nz, rows, width), bf),
            pltpu.VMEM((n_sp * nz, rows, width), bf),
            pltpu.VMEM((2, 2, nz, rows, half), bf),
            pltpu.VMEM((2, nz, rows, half), bf),
            pltpu.VMEM((nz, rows, width), bf),
            pltpu.VMEM(w_gate.shape, bf),
            pltpu.VMEM(w_up.shape, bf),
            pltpu.VMEM(w_down.shape, bf),
            dma((9,)), dma((4,)),
            dma((n_tp,)), dma((n_tp,)), dma, dma((3,)), dma((3,)),
            dma((nz,)), dma((nz,)), dma((2, nz)), dma((2, 2, nz)), dma((2, 4, nz)),
            dma((n_sp * nz,)), dma((n_sp * nz,)),
            dma((nz,)), dma((nz,)),
            dma((2, 2, nz)), dma((2, 2, nz)), dma((2, nz)), dma((2, nz)),
            dma((nz,)), dma((nz,)),
        ],
        compiler_params=pltpu.CompilerParams(
            collective_id=0, has_side_effects=True, vmem_limit_bytes=64000000
        ),
    )(*operands, w_out, w_gate, w_up, w_down)


def passed_along(block, axis, distance):
    devices = range(lax.axis_size(axis))
    route = [(i - distance, i) for i in devices if i - distance in devices]
    return lax.ppermute(block, axis, route)


def local(
    gate_b,
    gate_c,
    values_in,
    conv_w,
    documents,
    w_out,
    resid,
    norm_gain,
    route_ids,
    route_weight,
    w_gate,
    w_up,
    w_down,
):
    seq_rows = gate_b.shape[0]
    local_rows = resid.shape[0]
    model_width = resid.shape[1]
    experts = lax.axis_size("sp") * w_gate.shape[0]
    capacity = 4 * local_rows // experts
    if lax.axis_size("sp") == 4 and w_gate.shape[0] == 1 and capacity >= local_rows:
        return layer(
            gate_b, gate_c, values_in, conv_w, documents.reshape(-1, LANES), resid,
            norm_gain.reshape(-1, LANES), route_ids.T, route_weight.T,
            w_out, w_gate[0], w_up[0], w_down[0],
        )
    last_rows = jnp.stack([gate_c[seq_rows - 2 :], values_in[seq_rows - 2 :]])
    before, before_docs = passed_along((last_rows, documents[seq_rows - 2 :]), "sp", 1)
    products = jnp.concatenate(
        [
            before[0].astype(jnp.float32) * before[1].astype(jnp.float32),
            gate_c.astype(jnp.float32) * values_in.astype(jnp.float32),
        ],
        axis=0,
    )
    docs_all = jnp.concatenate([before_docs, documents], axis=0)
    kernel_taps = conv_w.astype(jnp.float32)
    near_mask = (docs_all[1:-1] == documents).astype(jnp.float32)[:, None]
    far_mask = (docs_all[:-2] == documents).astype(jnp.float32)[:, None]
    convolved = (
        kernel_taps[2] * products[2:]
        + kernel_taps[1] * products[1:-1] * near_mask
        + kernel_taps[0] * products[:-2] * far_mask
    )
    mixed_rows = (gate_b.astype(jnp.float32) * convolved).astype(jnp.bfloat16)
    token_rows = lax.all_to_all(mixed_rows, "tp", split_axis=0, concat_axis=1, tiled=True)
    projected = jnp.dot(token_rows, w_out, preferred_element_type=jnp.float32)
    hidden_state = (resid.astype(jnp.float32) + projected).astype(jnp.bfloat16)
    state_wide = hidden_state.astype(jnp.float32)
    normed = (
        state_wide
        * lax.rsqrt(jnp.mean(state_wide * state_wide, axis=-1, keepdims=True) + 1e-06)
        * norm_gain.astype(jnp.float32)
    ).astype(jnp.bfloat16)
    experts = lax.axis_size("sp") * w_gate.shape[0]
    capacity = 4 * local_rows // experts
    flat_ids = route_ids.reshape(-1)
    one_hot = (flat_ids[:, None] == jnp.arange(experts, dtype=jnp.int32)[None, :]).astype(jnp.int32)
    rank_in = jnp.sum((jnp.cumsum(one_hot, axis=0) - one_hot) * one_hot, axis=1)
    slot_index = flat_ids * capacity + rank_in
    placement = (
        slot_index[:, None] == jnp.arange(experts * capacity, dtype=jnp.int32)[None, :]
    ).astype(jnp.bfloat16)
    repeated = jnp.repeat(normed, 2, axis=0)
    dispatch = jnp.einsum(
        "js,jd->sd", placement, repeated, preferred_element_type=jnp.float32
    ).astype(jnp.bfloat16)
    dispatch = dispatch.reshape(experts, capacity, model_width)
    gathered_piece = lax.all_gather(
        lax.all_to_all(dispatch, "sp", split_axis=0, concat_axis=0, tiled=True),
        "tp",
        axis=0,
        tiled=True,
    )
    flat_rows = gathered_piece.reshape(-1, model_width)
    gate_part = jnp.dot(flat_rows, w_gate[0], preferred_element_type=jnp.float32)
    up_part = jnp.dot(flat_rows, w_up[0], preferred_element_type=jnp.float32)
    activated = (jax.nn.silu(gate_part) * up_part).astype(jnp.bfloat16)
    partial_value = jnp.dot(activated, w_down[0], preferred_element_type=jnp.float32)
    partial_value = partial_value.reshape(
        gathered_piece.shape[0], gathered_piece.shape[1], model_width
    )
    summed = lax.psum_scatter(
        partial_value.astype(jnp.bfloat16), "tp", scatter_dimension=0, tiled=True
    )
    returned = lax.all_to_all(summed, "sp", split_axis=0, concat_axis=0, tiled=True)
    picked = jnp.take(
        returned.reshape(experts * capacity, model_width), slot_index, axis=0
    ).reshape(local_rows, 2, model_width)
    combined = jnp.sum(route_weight[:, :, None] * picked.astype(jnp.float32), axis=1)
    return (hidden_state.astype(jnp.float32) + combined).astype(jnp.bfloat16)


def solution(mesh):
    return jax.shard_map(
        local,
        mesh=mesh,
        in_specs=(
            P("sp", "tp"),
            P("sp", "tp"),
            P("sp", "tp"),
            P(None, "tp"),
            P("sp"),
            P(),
            P(("sp", "tp"), None),
            P(),
            P(("sp", "tp"), None),
            P(("sp", "tp"), None),
            P("sp", None, "tp"),
            P("sp", None, "tp"),
            P("sp", "tp", None),
        ),
        out_specs=P(("sp", "tp"), None),
        check_vma=False,
    )
```

time: 125 us -> 102 us (0.82)
  the two profiles are of different devices: /device:TPU:10 before, /device:TPU:0 now
where the time goes in v1:
time: 102 us
  Pallas kernels  101 us (99%)
  local copies, waits for them, and re-layouts  1.67 us (2%)
    pallas_call x1, Pallas kernels, layer(): pl.pallas_call(moe_kernel, out_shape=jax.ShapeDtypeStruct((rows, width),...  101 us

profile of v1, /device:TPU:0, one launch (start us, length us, event | category | flops | bytes accessed | tf_op | source)
XLA Modules:
  0.0 102.2 jit_solution(16622931834890092134)
XLA Ops:
  0.0 100.6 %shard_map.127 = bf16[64,2048]{1,0:T(8,128)(2,1)} custom-call(bf16[512,128]{1,0:T(8,128)(2,1)} %gb_hbm.1, bf16[512,128]{1,0:T(8,128)(2,1)} %gc_hbm.1, bf16[512,128]{1,0:T(8,128)(2,1)} %vals_hbm.1, bf16[3,128]{1,0:T(4,128)(2,1)} %taps_hbm.1, s32[4,128]{1,0:T(4,128)} %bitcast.11, bf16[64,2048]{1,0:T(8,128)(2,1)} %resid_hbm.1, bf16[16,128]{1,0:T(8,128)(2,1)} %bitcast.10, ...), custom_call_target="tpu_custom_call" | custom-call | tf_op jit(solution)/shard_map/pallas_call | solution.py:452
  100.6 1.7 %copy.15 = bf16[64,2048]{1,0:T(8,128)(2,1)} copy(bf16[64,2048]{1,0:T(8,128)(2,1)} %shard_map.127) | data formatting | bytes 524288

commit v2 on v1

--- a/solution.py
+++ b/solution.py
@@ -16,11 +16,11 @@
     wo_hbm, wg_hbm, wu_hbm, wd_hbm, out_ref,
     gb, gc, vals, taps, docs, resid, gain, ids, route,
     hid, tok, mixed, pad, dpad, mat, hc, hv, hd, wo,
-    xbuf, pbuf, dbuf, r1, r2, rz, wg, wu, wd,
+    xbuf, pbuf, dbuf, r1, r2, rm, rz, wg, wu, wd,
     in_sem, w_sem,
     s_a, r_a, s_b, s_h, r_h3,
-    s_z, r_z, s_1, s_2, r_h, s_p, r_p,
-    s_d, r_d, s_r1, r_r1, s_r2, r_r2, s_rz, r_rz,
+    s_z, s_f, r_z, s_1, s_2, r_h, s_p, r_p,
+    s_d, r_d, s_r1, r_r1, s_r2, r_r2, s_m, r_m, s_rz, r_rz,
 ):
     f32 = jnp.float32
     n_sp, n_tp = lax.axis_size("sp"), lax.axis_size("tp")
@@ -39,6 +39,8 @@
     other = (sp, z * 2 + 1 - c)
     following, previous = (lax.rem(sp + 1, n_sp), tp), (lax.rem(sp + n_sp - 1, n_sp), tp)
     to_x, to_y = (xn, tp), (yn, tp)
+    inner = z % 2 != z // 2
+    outer = z % 2 == z // 2
 
     def zz(k):
         if k < 2:
@@ -175,6 +177,17 @@
         at = xbuf.at[c, slot(k, OWN)]
         return rc(at, at, s_z.at[k], r_z.at[zz(k)], (sp, zz(k) * 2 + c))
 
+    def forward(k):
+        at = xbuf.at[c, slot(k, OWN)]
+        return rc(at, at, s_f.at[k], r_z.at[zz(k)], (sp, zz(2 if k == 1 else 1) * 2 + c))
+
+    def pass_on(k):
+        @pl.when(inner)
+        def _():
+            if k > 1:
+                z_recv(k).wait_recv()
+            forward(k).start()
+
     def piece(h, rel, k, ss, there, dev):
         at = xbuf.at[c, slot(k, rel), :, lanes(h)]
         return rc(at, at, ss, r_h.at[h, there, k], dev)
@@ -203,7 +216,12 @@
         to_other(OWN, k).start()
 
     def take(k):
-        z_recv(k).wait_recv()
+        if k == 1:
+            z_recv(k).wait_recv()
+        else:
+            @pl.when(outer)
+            def _():
+                z_recv(k).wait_recv()
         spread(k)
 
     def relay(k):
@@ -244,13 +262,14 @@
         at = pbuf.at[c, slot(k, YN if h == 0 else XN), :, cols(h)]
         return rc(at, r2.at[h, k], s_r2.at[h, k], r_r2.at[h, k], to_y if h == 0 else to_x)
 
+    def mate_copy(k):
+        at = pbuf.at[c, slot(k, OWN)]
+        return rc(at, rm.at[k - 2], s_m.at[k - 2], r_m.at[k - 2], (sp, zz(1) * 2 + c))
+
     def rz_copy(k):
+        n = min(k - 1, 1)
         at = pbuf.at[c, slot(k, OWN)]
-        return rc(at, rz.at[z], s_rz.at[k], r_rz.at[z], (sp, zz(k) * 2 + c))
-
-    def rz_recv(k):
-        at = pbuf.at[c, slot(k, OWN)]
-        return rc(at, rz.at[zz(k)], s_rz.at[k], r_rz.at[zz(k)], (sp, zz(k) * 2 + c))
+        return rc(at, rz.at[n], s_rz.at[k], r_rz.at[n], (sp, zz(k) * 2 + c))
 
     def stage1(k, parts=(1, 0)):
         for o in parts:
@@ -278,7 +297,20 @@
     def stage3(k):
         for h in (0, 1):
             pbuf[c, slot(k, OWN), :, cols(h)] = summed(h, k).astype(pbuf.dtype)
-        rz_copy(k).start()
+        if k == 1:
+            rz_copy(k).start()
+        else:
+            @pl.when(outer)
+            def _():
+                mate_copy(k).start()
+
+    def stage4(k):
+        @pl.when(inner)
+        def _():
+            mate_copy(k).wait_recv()
+            at = slot(k, OWN)
+            pbuf[c, at] = (pbuf[c, at].astype(f32) + rm[k - 2].astype(f32)).astype(pbuf.dtype)
+            rz_copy(k).start()
 
     barrier = pltpu.get_barrier_semaphore()
     peers = [to_x, to_y, following, previous] + [(sp, lax.rem(tp + d, n_tp)) for d in range(1, n_tp)]
@@ -311,13 +343,19 @@
     mix()
     for h in (1, 0):
         first(h, 0).start()
-    for k in range(1, nz):
-        z_send(k).start()
+    z_send(1).start()
+
+    @pl.when(inner)
+    def _():
+        z_send(2).start()
+
     for h in (0, 1):
         second(h, 0).start()
     to_other(OWN, 0).start()
     relay(0)
     take(1)
+    pass_on(1)
+    pass_on(2)
     sides(0)
     corner(0)
     for w in weights:
@@ -333,6 +371,7 @@
         table.setdefault(s, []).append(functools.partial(work, *args))
 
     end = nz - 1
+    put(before, 2, pass_on, 3)
     for k in range(1, nz):
         put(before, 2 * k - 1, relay, k)
         if k < end:
@@ -341,11 +380,10 @@
         put(before, 2 * k, corner, k)
     for k in range(end - 1):
         put(after, 2 * k + 2, merge, k)
-        if k > 0:
-            put(before, 2 * k + 3, stage1, k)
+    put(before, 2 * end - 1, stage1, 1, (1,))
     put(before, 2 * end, merge, end - 1)
     put(before, 2 * end, stage1, end - 1)
-    put(before, 2 * end + 1, stage2, 1)
+    put(before, 2 * end + 1, stage2, end - 1)
 
     @pl.loop(0, steps)
     def _(s):
@@ -389,22 +427,20 @@
 
     merge(end)
     stage1(end)
-    for k in range(2, end):
-        stage2(k)
-    stage1(0, (1,))
+    stage3(end - 1)
+    stage2(end)
+    stage1(1, (0,))
+    stage2(1)
+    stage1(0)
+    stage4(end - 1)
+    stage3(end)
     stage3(1)
-    stage2(end)
-    stage1(0, (0,))
-    for k in range(2, end):
-        stage3(k)
-    stage3(end)
+    stage4(end)
     stage2(0)
+    rz_copy(1).wait_recv()
+    rz_copy(2).wait_recv()
     for h in (0, 1):
-        total = summed(h, 0)
-        for k in range(1, nz):
-            if h == 0:
-                rz_recv(k).wait_recv()
-            total = total + rz[zz(k), :, cols(h)].astype(f32)
+        total = summed(h, 0) + rz[0, :, cols(h)].astype(f32) + rz[1, :, cols(h)].astype(f32)
         out_ref[:, cols(h)] = (hid[:, cols(h)].astype(f32) + total).astype(out_ref.dtype)
 
     for copy in halo_copies():
@@ -418,9 +454,22 @@
     def _():
         swap_first().wait_send()
 
-    for k in range(1, nz):
-        z_send(k).wait_send()
-        rz_copy(k).wait_send()
+    z_send(1).wait_send()
+    rz_copy(1).wait_send()
+
+    @pl.when(inner)
+    def _():
+        z_send(2).wait_send()
+        for k in range(1, nz):
+            forward(k).wait_send()
+        for k in range(2, nz):
+            rz_copy(k).wait_send()
+
+    @pl.when(outer)
+    def _():
+        for k in range(2, nz):
+            mate_copy(k).wait_send()
+
     for k in range(nz):
         for h in (0, 1):
             first(h, k).wait_send()
@@ -451,7 +500,7 @@
     operands = (gate_b, gate_c, values_in, conv_w, docs, resid, gain, ids, route)
     return pl.pallas_call(
         moe_kernel,
-        out_shape=jax.ShapeDtypeStruct((rows, width), bf),
+        out_shape=pltpu.VMEM((rows, width), bf),
         in_specs=[hbm] * 13,
         out_specs=vmem,
         scratch_shapes=[pltpu.VMEM(a.shape, a.dtype) for a in operands] + [
@@ -470,17 +519,18 @@
             pltpu.VMEM((n_sp * nz, rows, width), bf),
             pltpu.VMEM((2, 2, nz, rows, half), bf),
             pltpu.VMEM((2, nz, rows, half), bf),
-            pltpu.VMEM((nz, rows, width), bf),
+            pltpu.VMEM((2, rows, width), bf),
+            pltpu.VMEM((2, rows, width), bf),
             pltpu.VMEM(w_gate.shape, bf),
             pltpu.VMEM(w_up.shape, bf),
             pltpu.VMEM(w_down.shape, bf),
             dma((9,)), dma((4,)),
             dma((n_tp,)), dma((n_tp,)), dma, dma((3,)), dma((3,)),
-            dma((nz,)), dma((nz,)), dma((2, nz)), dma((2, 2, nz)), dma((2, 4, nz)),
+            dma((nz,)), dma((nz,)), dma((nz,)), dma((2, nz)), dma((2, 2, nz)), dma((2, 4, nz)),
             dma((n_sp * nz,)), dma((n_sp * nz,)),
             dma((nz,)), dma((nz,)),
             dma((2, 2, nz)), dma((2, 2, nz)), dma((2, nz)), dma((2, nz)),
-            dma((nz,)), dma((nz,)),
+            dma((2,)), dma((2,)), dma((nz,)), dma((2,)),
         ],
         compiler_params=pltpu.CompilerParams(
             collective_id=0, has_side_effects=True, vmem_limit_bytes=64000000
@@ -514,7 +564,7 @@
     model_width = resid.shape[1]
     experts = lax.axis_size("sp") * w_gate.shape[0]
     capacity = 4 * local_rows // experts
-    if lax.axis_size("sp") == 4 and w_gate.shape[0] == 1 and capacity >= local_rows:
+    if (lax.axis_size("sp"), lax.axis_size("tp")) == (4, 8) and w_gate.shape[0] == 1 and capacity >= local_rows:
         return layer(
             gate_b, gate_c, values_in, conv_w, documents.reshape(-1, LANES), resid,
             norm_gain.reshape(-1, LANES), route_ids.T, route_weight.T,

time: 102 us -> 93.3 us (0.915)
  Pallas kernels: 101 us -> 92.4 us
    pallas_call x1, Pallas kernels: 101 us -> 92.4 us  [layer(): pl.pallas_call(moe_kernel, out_shape=pltpu.VMEM((rows, width), bf), in_sp...]
where the time goes in v2:
time: 93.3 us; the launch traced here: 93.2 us
  Pallas kernels  92.4 us (99%)
    pallas_call x1, Pallas kernels, layer(): pl.pallas_call(moe_kernel, out_shape=pltpu.VMEM((rows, width), bf), in_sp...  92.4 us

profile of v2, /device:TPU:0, one launch (start us, length us, event | category | flops | bytes accessed | tf_op | source)
XLA Modules:
  0.0 93.2 jit_solution(9416776513969537421)
XLA Ops:
  0.0 92.4 %shard_map.127 = bf16[64,2048]{1,0:T(8,128)(2,1)S(1)} custom-call(bf16[512,128]{1,0:T(8,128)(2,1)} %gb_hbm.1, bf16[512,128]{1,0:T(8,128)(2,1)} %gc_hbm.1, bf16[512,128]{1,0:T(8,128)(2,1)} %vals_hbm.1, bf16[3,128]{1,0:T(4,128)(2,1)} %taps_hbm.1, s32[4,128]{1,0:T(4,128)} %bitcast.11, bf16[64,2048]{1,0:T(8,128)(2,1)} %resid_hbm.1, bf16[16,128]{1,0:T(8,128)(2,1)} %bitcast.10, ...), custom_call_target="tpu_custom_call" | custom-call | tf_op jit(solution)/shard_map/pallas_call | solution.py:501
  92.4 0.7 copy.15

commit v3 on v2

--- a/solution.py
+++ b/solution.py
@@ -15,12 +15,13 @@
     gb_hbm, gc_hbm, vals_hbm, taps_hbm, docs_hbm, resid_hbm, gain_hbm, ids_hbm, route_hbm,
     wo_hbm, wg_hbm, wu_hbm, wd_hbm, out_ref,
     gb, gc, vals, taps, docs, resid, gain, ids, route,
-    hid, tok, mixed, pad, dpad, mat, hc, hv, hd, wo,
-    xbuf, pbuf, dbuf, r1, r2, rm, rz, wg, wu, wd,
+    hid, tok, mixed, pad, dpad, mat, hc, hv, hd, wo, named, shares, table, turned_table,
+    xbuf, pbuf, dbuf, r1, r2, rm, rz, rbz, rbp, acts, wg, wu, wd,
     in_sem, w_sem,
-    s_a, r_a, s_b, s_h, r_h3,
+    s_a, r_a, s_b, s_h, r_h3, s_n, r_n, s_t, r_t,
     s_z, s_f, r_z, s_1, s_2, r_h, s_p, r_p,
     s_d, r_d, s_r1, r_r1, s_r2, r_r2, s_m, r_m, s_rz, r_rz,
+    s_bz, r_bz, s_bp, r_bp, s_ap, r_ap, s_az, r_az, s_ao, r_ao,
 ):
     f32 = jnp.float32
     n_sp, n_tp = lax.axis_size("sp"), lax.axis_size("tp")
@@ -50,11 +51,17 @@
     def slot(k, rel):
         return zz(k) * n_sp + columns[rel]
 
-    def lanes(h):
-        return pl.ds(0, half) if h == 0 else pl.ds(half, xbuf.shape[3] - half)
-
     def cols(h):
         return pl.ds(h * half, half)
+
+    quarter = rbz.shape[3]
+    share = (width - quarter) // 2
+
+    def part(h):
+        return pl.ds(h * share, share)
+
+    body = pl.ds(0, 2 * share)
+    along = pl.ds(2 * share, quarter)
 
     def rc(src, dst, ss, rs, dev):
         return pltpu.make_async_remote_copy(
@@ -87,6 +94,36 @@
 
     def swap_first():
         return rc(token_rows(0), tok.at[:, channels(tp)], s_b, r_a.at[tp], (sp, 0))
+
+
+    def name_copy(rel):
+        return rc(named.at[columns[rel]], shares.at[sp], s_n.at[rel], r_n.at[rel], (columns[rel], tp))
+
+    def table_copy(d):
+        return rc(shares, table.at[tp], s_t.at[d], r_t.at[tp], (sp, lax.rem(tp + d, n_tp)))
+
+    def table_recv(d):
+        j = lax.rem(tp + d, n_tp)
+        return rc(shares, table.at[j], s_t.at[d], r_t.at[j], (sp, j))
+
+    def name():
+        named[...] = jnp.zeros_like(named)
+        for e in range(n_sp):
+            named[e, :, pl.ds(0, rows)] = jnp.where(ids[0:1] == e, route[0:1], 0.0) + jnp.where(
+                ids[1:2] == e, route[1:2], 0.0
+            )
+        for rel in (XN, YN, DG):
+            name_copy(rel).start()
+        shares[sp] = named[sp]
+
+    def tabulate():
+        for d in range(1, n_tp):
+            table_recv(d).wait_recv()
+        mat[...] = jnp.zeros_like(mat)
+        for j in range(n_tp):
+            for e in range(n_sp):
+                mat[pl.ds(j * n_sp + e, 1)] = table[j, e]
+        turned_table[...] = mat[...].T
 
     def convolve(first, count):
         own = pl.ds(first, count)
@@ -102,11 +139,9 @@
         mixed[own] = (gb[own].astype(f32) * convolved).astype(mixed.dtype)
 
     def mix():
+        doc_rows = docs.shape[0]
         mat[...] = jnp.zeros_like(mat)
-        doc_rows = docs.shape[0]
         mat[pl.ds(0, doc_rows)] = docs[...].astype(f32)
-        mat[pl.ds(doc_rows, 2), pl.ds(0, rows)] = ids[...].astype(f32)
-        mat[pl.ds(doc_rows + 2, 2), pl.ds(0, rows)] = route[...]
         turned = mat[...].T
         for n in range(doc_rows):
             dpad[pl.ds(8 + n * LANES, LANES)] = jnp.broadcast_to(
@@ -121,20 +156,7 @@
             def _():
                 swap(d).start()
 
-        lane = lax.broadcasted_iota(jnp.int32, (rows, LANES), 1)
-        named = (lane % n_sp).astype(f32)
-        part = lane // n_sp
-        side = turned[:rows]
-        at = doc_rows
-        share = jnp.where(side[:, at : at + 1] == named, side[:, at + 2 : at + 3], 0.0) + jnp.where(
-            side[:, at + 1 : at + 2] == named, side[:, at + 3 : at + 4], 0.0
-        )
-        high = share.astype(jnp.bfloat16).astype(f32)
-        middle = (share - high).astype(jnp.bfloat16).astype(f32)
-        low = share - high - middle
-        terms = jnp.where(part == 0, high, jnp.where(part == 1, middle, jnp.where(part == 2, low, 0.0)))
         mine = z * n_sp + sp
-        xbuf[c, mine, :, pl.ds(width, LANES)] = terms.astype(xbuf.dtype)
 
         for copy in halo_copies():
             copy.wait_recv()
@@ -150,6 +172,12 @@
         @pl.when(tp != 0)
         def _():
             swap_first().start()
+
+        for rel in (XN, YN, DG):
+            name_copy(rel).wait_recv()
+        table[tp] = shares[...]
+        for d in range(1, n_tp):
+            table_copy(d).start()
 
         tok[:, channels(tp)] = mixed[pl.ds(pl.multiple_of(tp * rows, rows), rows)]
         in_copies[5].wait()
@@ -170,15 +198,15 @@
 
 
     def z_send(k):
-        at = xbuf.at[c, z * n_sp + sp]
+        at = xbuf.at[c, z * n_sp + sp, :, body]
         return rc(at, at, s_z.at[k], r_z.at[z], (sp, zz(k) * 2 + c))
 
     def z_recv(k):
-        at = xbuf.at[c, slot(k, OWN)]
+        at = xbuf.at[c, slot(k, OWN), :, body]
         return rc(at, at, s_z.at[k], r_z.at[zz(k)], (sp, zz(k) * 2 + c))
 
     def forward(k):
-        at = xbuf.at[c, slot(k, OWN)]
+        at = xbuf.at[c, slot(k, OWN), :, body]
         return rc(at, at, s_f.at[k], r_z.at[zz(k)], (sp, zz(2 if k == 1 else 1) * 2 + c))
 
     def pass_on(k):
@@ -189,7 +217,7 @@
             forward(k).start()
 
     def piece(h, rel, k, ss, there, dev):
-        at = xbuf.at[c, slot(k, rel), :, lanes(h)]
+        at = xbuf.at[c, slot(k, rel), :, part(h)]
         return rc(at, at, ss, r_h.at[h, there, k], dev)
 
     def first(h, k):
@@ -205,8 +233,29 @@
         piece(h, rel, k, s_1.at[h, k], rel, other).wait_recv()
 
     def to_other(rel, k):
-        at = xbuf.at[c, slot(k, rel)]
+        at = xbuf.at[c, slot(k, rel), :, body]
         return rc(at, at, s_p.at[k * n_sp + rel], r_p.at[k * n_sp + rel], other)
+
+
+    def ap_copy(rel):
+        at = xbuf.at[c, z * n_sp + sp, :, along]
+        return rc(at, at, s_ap.at[rel], r_ap.at[rel], (columns[rel], tp))
+
+    def ap_recv(rel):
+        at = xbuf.at[c, slot(0, rel), :, along]
+        return rc(at, at, s_ap.at[rel], r_ap.at[rel], (columns[rel], tp))
+
+    def az_copy(k):
+        at = xbuf.at[c, pl.ds(z * n_sp, n_sp), :, along]
+        return rc(at, at, s_az.at[k], r_az.at[z], (sp, zz(k) * 2 + c))
+
+    def az_recv(k):
+        at = xbuf.at[c, group(k), :, along]
+        return rc(at, at, s_az.at[k], r_az.at[zz(k)], (sp, zz(k) * 2 + c))
+
+    def ao_copy(k):
+        at = xbuf.at[c, group(k), :, along]
+        return rc(at, at, s_ao.at[k], r_ao.at[k], other)
 
     def spread(k):
         for h in (1, 0):
@@ -231,6 +280,9 @@
         third(1, k).start()
 
     def sides(k):
+        if k > 0:
+            az_recv(k).wait_recv()
+            ao_copy(k).start()
         arrived(0, XN, k)
         to_other(XN, k).start()
         arrived(1, YN, k)
@@ -245,31 +297,65 @@
     def group(k):
         return pl.ds(zz(k) * n_sp, n_sp)
 
-    def d_copy(k):
-        return rc(pbuf.at[1 - c, group(k)], dbuf.at[group(k)], s_d.at[k], r_d.at[k], other)
-
-    def merge(k):
-        d_copy(k).wait_recv()
-        i = group(k)
+    def couple(at_z, s):
+        row = y + s % 2 - 2 * y * (s % 2)
+        return pl.ds(at_z * n_sp + 2 * row, 2)
+
+    def d_copy(s):
+        i = couple(zz(s // 2), s)
+        return rc(pbuf.at[1 - c, i], dbuf.at[i], s_d.at[s], r_d.at[s], other)
+
+    def merge(s):
+        d_copy(s).wait_recv()
+        i = couple(zz(s // 2), s)
         pbuf[c, i] = (pbuf[c, i].astype(f32) + dbuf[i].astype(f32)).astype(pbuf.dtype)
+
+    def spread_along(k):
+        bz_copy(k).start()
 
     def r1_copy(h, o, k):
         rel = DG if o else (XN if h == 0 else YN)
-        at = pbuf.at[c, slot(k, rel), :, cols(h)]
+        at = pbuf.at[c, slot(k, rel), :, part(h)]
         return rc(at, r1.at[h, o, k], s_r1.at[h, o, k], r_r1.at[h, o, k], to_x if h == 0 else to_y)
 
     def r2_copy(h, k):
-        at = pbuf.at[c, slot(k, YN if h == 0 else XN), :, cols(h)]
+        at = pbuf.at[c, slot(k, YN if h == 0 else XN), :, part(h)]
         return rc(at, r2.at[h, k], s_r2.at[h, k], r_r2.at[h, k], to_y if h == 0 else to_x)
 
-    def mate_copy(k):
-        at = pbuf.at[c, slot(k, OWN)]
-        return rc(at, rm.at[k - 2], s_m.at[k - 2], r_m.at[k - 2], (sp, zz(1) * 2 + c))
-
-    def rz_copy(k):
+    def mate_copy(h, k):
+        at = pbuf.at[c, slot(k, OWN), :, part(h)]
+        return rc(at, rm.at[k - 2, :, part(h)], s_m.at[k - 2, h], r_m.at[k - 2, h], (sp, zz(1) * 2 + c))
+
+    def rz_copy(h, k):
         n = min(k - 1, 1)
-        at = pbuf.at[c, slot(k, OWN)]
-        return rc(at, rz.at[n], s_rz.at[k], r_rz.at[n], (sp, zz(k) * 2 + c))
+        at = pbuf.at[c, slot(k, OWN), :, part(h)]
+        return rc(at, rz.at[n, :, part(h)], s_rz.at[k, h], r_rz.at[n, h], (sp, zz(k) * 2 + c))
+
+    def bz_copy(k):
+        return rc(
+            pbuf.at[c, group(k), :, along], rbz.at[z], s_bz.at[k], r_bz.at[z], (sp, zz(k) * 2 + c)
+        )
+
+    def bz_recv(k):
+        return rc(
+            pbuf.at[c, group(k), :, along], rbz.at[zz(k)], s_bz.at[k], r_bz.at[zz(k)],
+            (sp, zz(k) * 2 + c),
+        )
+
+    def bp_copy(rel):
+        return rc(
+            pbuf.at[c, slot(0, rel), :, along], rbp.at[rel], s_bp.at[rel], r_bp.at[rel],
+            (columns[rel], tp),
+        )
+
+    def along_sum():
+        total = pbuf[c, group(0), :, along].astype(f32)
+        for k in range(1, nz):
+            bz_recv(k).wait_recv()
+            total = total + rbz[zz(k)].astype(f32)
+        pbuf[c, group(0), :, along] = total.astype(pbuf.dtype)
+        for rel in (DG, XN, YN):
+            bp_copy(rel).start()
 
     def stage1(k, parts=(1, 0)):
         for o in parts:
@@ -280,8 +366,8 @@
         for h in (0, 1):
             r1_copy(h, 1, k).wait_recv()
             i = slot(k, YN if h == 0 else XN)
-            pbuf[c, i, :, cols(h)] = (
-                pbuf[c, i, :, cols(h)].astype(f32) + r1[h, 1, k].astype(f32)
+            pbuf[c, i, :, part(h)] = (
+                pbuf[c, i, :, part(h)].astype(f32) + r1[h, 1, k].astype(f32)
             ).astype(pbuf.dtype)
             r2_copy(h, k).start()
 
@@ -289,31 +375,34 @@
         r1_copy(h, 0, k).wait_recv()
         r2_copy(h, k).wait_recv()
         return (
-            pbuf[c, slot(k, OWN), :, cols(h)].astype(f32)
+            pbuf[c, slot(k, OWN), :, part(h)].astype(f32)
             + r1[h, 0, k].astype(f32)
             + r2[h, k].astype(f32)
         )
 
     def stage3(k):
         for h in (0, 1):
-            pbuf[c, slot(k, OWN), :, cols(h)] = summed(h, k).astype(pbuf.dtype)
-        if k == 1:
-            rz_copy(k).start()
-        else:
-            @pl.when(outer)
-            def _():
-                mate_copy(k).start()
+            pbuf[c, slot(k, OWN), :, part(h)] = summed(h, k).astype(pbuf.dtype)
+            if k == 1:
+                rz_copy(h, k).start()
+            else:
+                @pl.when(outer)
+                def _():
+                    mate_copy(h, k).start()
 
     def stage4(k):
         @pl.when(inner)
         def _():
-            mate_copy(k).wait_recv()
             at = slot(k, OWN)
-            pbuf[c, at] = (pbuf[c, at].astype(f32) + rm[k - 2].astype(f32)).astype(pbuf.dtype)
-            rz_copy(k).start()
+            for h in (0, 1):
+                mate_copy(h, k).wait_recv()
+                pbuf[c, at, :, part(h)] = (
+                    pbuf[c, at, :, part(h)].astype(f32) + rm[k - 2, :, part(h)].astype(f32)
+                ).astype(pbuf.dtype)
+                rz_copy(h, k).start()
 
     barrier = pltpu.get_barrier_semaphore()
-    peers = [to_x, to_y, following, previous] + [(sp, lax.rem(tp + d, n_tp)) for d in range(1, n_tp)]
+    peers = [to_x, to_y, (dg, tp), following, previous] + [(sp, lax.rem(tp + d, n_tp)) for d in range(1, n_tp)]
     for peer in peers:
         pl.semaphore_signal(barrier, inc=1, device_id=peer, device_id_type=MESH)
     in_copies = [
@@ -340,7 +429,10 @@
         copy.start()
     for n in (3, 4, 7, 8):
         in_copies[n].wait()
+    name()
     mix()
+    for rel in (DG, XN, YN):
+        ap_copy(rel).start()
     for h in (1, 0):
         first(h, 0).start()
     z_send(1).start()
@@ -352,38 +444,49 @@
     for h in (0, 1):
         second(h, 0).start()
     to_other(OWN, 0).start()
+    for rel in (XN, YN, DG):
+        ap_recv(rel).wait_recv()
+    az_copy(1).start()
+    ao_copy(0).start()
     relay(0)
     take(1)
     pass_on(1)
     pass_on(2)
+    az_copy(2).start()
+    az_copy(3).start()
     sides(0)
-    corner(0)
+    tabulate()
     for w in weights:
         w.wait()
 
-    lane = lax.broadcasted_iota(jnp.int32, (1, LANES), 1)
-    chosen = ((lane % n_sp == sp) & (lane < 3 * n_sp)).astype(f32)
-
+    lane = lax.broadcasted_iota(jnp.int32, (rows, LANES), 1)
     steps = 2 * nz
-    before, after = {}, {}
+    before, middle, after = {}, {}, {}
 
     def put(table, s, work, *args):
         table.setdefault(s, []).append(functools.partial(work, *args))
 
     end = nz - 1
-    put(before, 2, pass_on, 3)
+    put(before, 1, relay, 1)
+    put(middle, 0, corner, 0)
+    put(middle, 1, pass_on, end)
     for k in range(1, nz):
-        put(before, 2 * k - 1, relay, k)
         if k < end:
-            put(before, 2 * k, take, k + 1)
-        put(before, 2 * k, sides, k)
-        put(before, 2 * k, corner, k)
-    for k in range(end - 1):
-        put(after, 2 * k + 2, merge, k)
-    put(before, 2 * end - 1, stage1, 1, (1,))
-    put(before, 2 * end, merge, end - 1)
-    put(before, 2 * end, stage1, end - 1)
-    put(before, 2 * end + 1, stage2, end - 1)
+            put(middle, 2 * k - 1, take, k + 1)
+            put(middle, 2 * k, relay, k + 1)
+        else:
+            put(middle, 2 * k, stage2, 1)
+        put(middle, 2 * k - 1, sides, k)
+        put(middle, 2 * k, corner, k)
+    for s in range(1, 2 * end):
+        put(after, s, merge, s - 1)
+    for k in range(1, end - 1):
+        put(after, 2 * k + 2, spread_along, k)
+    put(before, 2 * end - 1, stage1, 1)
+    put(middle, 2 * end, merge, 2 * end - 1)
+    put(middle, 2 * end, stage1, end - 1)
+    put(middle, 2 * end, spread_along, end - 1)
+    put(middle, 2 * end + 1, merge, 2 * end)
 
     @pl.loop(0, steps)
     def _(s):
@@ -394,30 +497,50 @@
                     work()
 
         k = s // 2
-        shared = (s + k // (nz - 1)) % 2
-        core = (c + shared) % 2
+        side = s % 2
         at_z = jnp.where(k < 2, 2 * (z // 2) + (z + k) % 2, k + (z // 2) * (nz - 1 - 2 * k))
-        i = pl.ds(at_z * n_sp, n_sp)
-
-        @pl.when(shared == 1)
+        for b in (0, 1):
+            column = jnp.where(side == 0, columns[b], columns[2 + b])
+            at = xbuf.at[1 - c, at_z * n_sp + column, :, body]
+            n = k * n_sp + 2 * side + b
+            rc(at, at, s_p.at[n], r_p.at[n], other).wait_recv()
+
+        @pl.when(side == 0)
         def _():
-            for rel in range(n_sp):
-                at = xbuf.at[1 - c, at_z * n_sp + rel]
-                n = k * n_sp + rel
-                rc(at, at, s_p.at[n], r_p.at[n], other).wait_recv()
-
-        held = xbuf[core, i].reshape(n_sp * rows, xbuf.shape[3])
-        scale = jnp.sum(held[:, width:].astype(f32) * chosen, axis=1, keepdims=True)
-        held = held[:, :width]
+            at = xbuf.at[1 - c, pl.ds(at_z * n_sp, n_sp), :, along]
+            rc(at, at, s_ao.at[k], r_ao.at[k], other).wait_recv()
+
+        i = couple(at_z, s)
+        held = xbuf[:, i].reshape(4 * rows, width)
+        row = y + side - 2 * y * side
+        scale = jnp.concatenate(
+            [
+                jnp.sum(
+                    jnp.where(
+                        lane == (at_z * 2 + core) * n_sp + 2 * row + e,
+                        turned_table[pl.ds(0, rows)], 0.0,
+                    ),
+                    axis=1,
+                    keepdims=True,
+                )
+                for core in (0, 1)
+                for e in (0, 1)
+            ],
+            axis=0,
+        )
         gate = jnp.dot(held, wg[...], preferred_element_type=f32)
         up = jnp.dot(held, wu[...], preferred_element_type=f32)
-        act = (jax.nn.silu(gate) * up * scale).astype(jnp.bfloat16)
-        down = jnp.dot(act, wd[...], preferred_element_type=f32)
-        pbuf[core, i] = down.astype(pbuf.dtype).reshape(n_sp, rows, width)
-
-        @pl.when(shared == 1)
-        def _():
-            rc(pbuf.at[1 - c, i], dbuf.at[i], s_d.at[k], r_d.at[k], other).start()
+        acts[...] = (jax.nn.silu(gate) * up * scale).astype(acts.dtype)
+
+        for at, works in middle.items():
+            @pl.when(s == at)
+            def _():
+                for work in works:
+                    work()
+
+        down = jnp.dot(acts[...], wd[...], preferred_element_type=f32)
+        pbuf[:, i] = down.astype(pbuf.dtype).reshape(2, 2, rows, width)
+        rc(pbuf.at[1 - c, i], dbuf.at[i], s_d.at[s], r_d.at[s], other).start()
 
         for at, works in after.items():
             @pl.when(s == at)
@@ -425,23 +548,30 @@
                 for work in works:
                     work()
 
-    merge(end)
+    stage3(1)
+    stage2(end - 1)
+    merge(2 * end + 1)
     stage1(end)
     stage3(end - 1)
+    spread_along(end)
     stage2(end)
-    stage1(1, (0,))
-    stage2(1)
     stage1(0)
     stage4(end - 1)
     stage3(end)
-    stage3(1)
+    stage2(0)
+    along_sum()
     stage4(end)
-    stage2(0)
-    rz_copy(1).wait_recv()
-    rz_copy(2).wait_recv()
     for h in (0, 1):
-        total = summed(h, 0) + rz[0, :, cols(h)].astype(f32) + rz[1, :, cols(h)].astype(f32)
-        out_ref[:, cols(h)] = (hid[:, cols(h)].astype(f32) + total).astype(out_ref.dtype)
+        total = hid[:, part(h)].astype(f32) + summed(h, 0)
+        for n in (0, 1):
+            rz_copy(h, n + 1).wait_recv()
+            total = total + rz[n, :, part(h)].astype(f32)
+        out_ref[:, part(h)] = total.astype(out_ref.dtype)
+    total = hid[:, along].astype(f32) + pbuf[c, slot(0, OWN), :, along].astype(f32)
+    for rel in (XN, YN, DG):
+        bp_copy(rel).wait_recv()
+        total = total + rbp[rel].astype(f32)
+    out_ref[:, along] = total.astype(out_ref.dtype)
 
     for copy in halo_copies():
         copy.wait_send()
@@ -454,8 +584,20 @@
     def _():
         swap_first().wait_send()
 
+    for rel in (XN, YN, DG):
+        name_copy(rel).wait_send()
+        bp_copy(rel).wait_send()
+        ap_copy(rel).wait_send()
+    for k in range(1, nz):
+        bz_copy(k).wait_send()
+        az_copy(k).wait_send()
+    for k in range(nz):
+        ao_copy(k).wait_send()
+    for d in range(1, n_tp):
+        table_copy(d).wait_send()
     z_send(1).wait_send()
-    rz_copy(1).wait_send()
+    for h in (0, 1):
+        rz_copy(h, 1).wait_send()
 
     @pl.when(inner)
     def _():
@@ -463,12 +605,14 @@
         for k in range(1, nz):
             forward(k).wait_send()
         for k in range(2, nz):
-            rz_copy(k).wait_send()
+            for h in (0, 1):
+                rz_copy(h, k).wait_send()
 
     @pl.when(outer)
     def _():
         for k in range(2, nz):
-            mate_copy(k).wait_send()
+            for h in (0, 1):
+                mate_copy(h, k).wait_send()
 
     for k in range(nz):
         for h in (0, 1):
@@ -480,18 +624,18 @@
             r2_copy(h, k).wait_send()
         for rel in range(n_sp):
             to_other(rel, k).wait_send()
-    for k in range(nz):
-        d_copy(k).wait_send()
+    for s in range(steps):
+        d_copy(s).wait_send()
 
 
 def layer(gate_b, gate_c, values_in, conv_w, docs, resid, gain, ids, route, w_out, w_gate, w_up, w_down):
     rows, width = resid.shape
-    wide = width + LANES
     seq, held = gate_b.shape
     n_tp = lax.axis_size("tp")
     n_sp = lax.axis_size("sp")
     nz = n_tp // 2
-    half = width // 2
+    quarter = width // 8
+    share = (width - quarter) // 2
     bf = jnp.bfloat16
     f32 = jnp.float32
     dma = pltpu.SemaphoreType.DMA
@@ -514,23 +658,33 @@
             pltpu.VMEM((16, held), bf),
             pltpu.VMEM(docs.shape, docs.dtype),
             pltpu.VMEM(w_out.shape, bf),
-            pltpu.VMEM((2, n_sp * nz, rows, wide), bf),
+            pltpu.VMEM((n_sp, 1, LANES), f32),
+            pltpu.VMEM((n_sp, 1, LANES), f32),
+            pltpu.VMEM((n_tp, n_sp, 1, LANES), f32),
+            pltpu.VMEM((LANES, LANES), f32),
+            pltpu.VMEM((2, n_sp * nz, rows, width), bf),
             pltpu.VMEM((2, n_sp * nz, rows, width), bf),
             pltpu.VMEM((n_sp * nz, rows, width), bf),
-            pltpu.VMEM((2, 2, nz, rows, half), bf),
-            pltpu.VMEM((2, nz, rows, half), bf),
-            pltpu.VMEM((2, rows, width), bf),
-            pltpu.VMEM((2, rows, width), bf),
+            pltpu.VMEM((2, 2, nz, rows, share), bf),
+            pltpu.VMEM((2, nz, rows, share), bf),
+            pltpu.VMEM((2, rows, 2 * share), bf),
+            pltpu.VMEM((2, rows, 2 * share), bf),
+            pltpu.VMEM((nz, n_sp, rows, quarter), bf),
+            pltpu.VMEM((4, rows, quarter), bf),
+            pltpu.VMEM((4 * rows, w_gate.shape[1]), bf),
             pltpu.VMEM(w_gate.shape, bf),
             pltpu.VMEM(w_up.shape, bf),
             pltpu.VMEM(w_down.shape, bf),
             dma((9,)), dma((4,)),
             dma((n_tp,)), dma((n_tp,)), dma, dma((3,)), dma((3,)),
+            dma((4,)), dma((4,)), dma((n_tp,)), dma((n_tp,)),
             dma((nz,)), dma((nz,)), dma((nz,)), dma((2, nz)), dma((2, 2, nz)), dma((2, 4, nz)),
             dma((n_sp * nz,)), dma((n_sp * nz,)),
-            dma((nz,)), dma((nz,)),
+            dma((2 * nz,)), dma((2 * nz,)),
             dma((2, 2, nz)), dma((2, 2, nz)), dma((2, nz)), dma((2, nz)),
-            dma((2,)), dma((2,)), dma((nz,)), dma((2,)),
+            dma((2, 2)), dma((2, 2)), dma((nz, 2)), dma((2, 2)),
+            dma((nz,)), dma((nz,)), dma((4,)), dma((4,)),
+            dma((4,)), dma((4,)), dma((nz,)), dma((nz,)), dma((nz,)), dma((nz,)),
         ],
         compiler_params=pltpu.CompilerParams(
             collective_id=0, has_side_effects=True, vmem_limit_bytes=64000000

time: 93.3 us -> 87.9 us (0.942)
  Pallas kernels: 92.4 us -> 87.1 us
    pallas_call x1, Pallas kernels: 92.4 us -> 87.1 us  [layer(): pl.pallas_call(moe_kernel, out_shape=pltpu.VMEM((rows, width), bf), in_sp...]
where the time goes in v3:
time: 87.9 us; the launch traced here: 87.8 us
  Pallas kernels  87.1 us (99%)
    pallas_call x1, Pallas kernels, layer(): pl.pallas_call(moe_kernel, out_shape=pltpu.VMEM((rows, width), bf), in_sp...  87.1 us

profile of v3, /device:TPU:0, one launch (start us, length us, event | category | flops | bytes accessed | tf_op | source)
XLA Modules:
  0.0 87.8 jit_solution(17902716275003800389)
XLA Ops:
  0.0 87.1 %shard_map.127 = bf16[64,2048]{1,0:T(8,128)(2,1)S(1)} custom-call(bf16[512,128]{1,0:T(8,128)(2,1)} %gb_hbm.1, bf16[512,128]{1,0:T(8,128)(2,1)} %gc_hbm.1, bf16[512,128]{1,0:T(8,128)(2,1)} %vals_hbm.1, bf16[3,128]{1,0:T(4,128)(2,1)} %taps_hbm.1, s32[4,128]{1,0:T(4,128)} %bitcast.11, bf16[64,2048]{1,0:T(8,128)(2,1)} %resid_hbm.1, bf16[16,128]{1,0:T(8,128)(2,1)} %bitcast.10, ...), custom_call_target="tpu_custom_call" | custom-call | tf_op jit(solution)/shard_map/pallas_call | solution.py:645
  87.1 0.7 copy.15

commit v4 on v3

--- a/solution.py
+++ b/solution.py
@@ -18,7 +18,7 @@
     hid, tok, mixed, pad, dpad, mat, hc, hv, hd, wo, named, shares, table, turned_table,
     xbuf, pbuf, dbuf, r1, r2, rm, rz, rbz, rbp, acts, wg, wu, wd,
     in_sem, w_sem,
-    s_a, r_a, s_b, s_h, r_h3, s_n, r_n, s_t, r_t,
+    s_a, r_a, s_h, r_h3, s_n, r_n, s_t, r_t,
     s_z, s_f, r_z, s_1, s_2, r_h, s_p, r_p,
     s_d, r_d, s_r1, r_r1, s_r2, r_r2, s_m, r_m, s_rz, r_rz,
     s_bz, r_bz, s_bp, r_bp, s_ap, r_ap, s_az, r_az, s_ao, r_ao,
@@ -86,25 +86,25 @@
 
     def swap(d):
         j = lax.rem(tp + d, n_tp)
-        return rc(token_rows(j), tok.at[:, channels(tp)], s_a.at[d], r_a.at[tp], (sp, j))
-
-    def swapped(d):
-        j = lax.rem(tp + d, n_tp)
-        return rc(token_rows(j), tok.at[:, channels(j)], s_a.at[d], r_a.at[j], (sp, j))
+        return rc(token_rows(j), tok.at[:, channels(tp)], s_a, r_a, (sp, j))
+
+    def swaps():
+        at = tok.at[:, pl.ds(0, (n_tp - 1) * gb.shape[1])]
+        return rc(at, at, s_a, r_a, other)
 
     def swap_first():
-        return rc(token_rows(0), tok.at[:, channels(tp)], s_b, r_a.at[tp], (sp, 0))
+        return rc(token_rows(0), tok.at[:, channels(tp)], s_a, r_a, (sp, 0))
 
 
     def name_copy(rel):
-        return rc(named.at[columns[rel]], shares.at[sp], s_n.at[rel], r_n.at[rel], (columns[rel], tp))
+        return rc(named.at[columns[rel]], shares.at[sp], s_n, r_n.at[rel], (columns[rel], tp))
 
     def table_copy(d):
-        return rc(shares, table.at[tp], s_t.at[d], r_t.at[tp], (sp, lax.rem(tp + d, n_tp)))
-
-    def table_recv(d):
-        j = lax.rem(tp + d, n_tp)
-        return rc(shares, table.at[j], s_t.at[d], r_t.at[j], (sp, j))
+        return rc(shares, table.at[tp], s_t, r_t, (sp, lax.rem(tp + d, n_tp)))
+
+    def tables():
+        at = table.at[pl.ds(0, n_tp - 1)]
+        return rc(at, at, s_t, r_t, other)
 
     def name():
         named[...] = jnp.zeros_like(named)
@@ -117,8 +117,7 @@
         shares[sp] = named[sp]
 
     def tabulate():
-        for d in range(1, n_tp):
-            table_recv(d).wait_recv()
+        tables().wait_recv()
         mat[...] = jnp.zeros_like(mat)
         for j in range(n_tp):
             for e in range(n_sp):
@@ -183,8 +182,7 @@
         in_copies[5].wait()
         in_copies[6].wait()
         wo_copy.wait()
-        for d in range(1, n_tp):
-            swapped(d).wait_recv()
+        swaps().wait_recv()
         projected = jnp.dot(tok[...], wo[...], preferred_element_type=f32)
         hidden = (resid[...].astype(f32) + projected).astype(hid.dtype)
         hid[...] = hidden
@@ -221,41 +219,41 @@
         return rc(at, at, ss, r_h.at[h, there, k], dev)
 
     def first(h, k):
-        return piece(h, OWN, k, s_1.at[h, k], YN if h == 0 else XN, to_y if h == 0 else to_x)
+        return piece(h, OWN, k, s_1, YN if h == 0 else XN, to_y if h == 0 else to_x)
 
     def second(h, k):
-        return piece(h, OWN, k, s_2.at[h, 0, k], XN if h == 0 else YN, to_x if h == 0 else to_y)
+        return piece(h, OWN, k, s_2, XN if h == 0 else YN, to_x if h == 0 else to_y)
 
     def third(h, k):
-        return piece(h, YN if h == 0 else XN, k, s_2.at[h, 1, k], DG, to_x if h == 0 else to_y)
+        return piece(h, YN if h == 0 else XN, k, s_2, DG, to_x if h == 0 else to_y)
 
     def arrived(h, rel, k):
-        piece(h, rel, k, s_1.at[h, k], rel, other).wait_recv()
+        piece(h, rel, k, s_1, rel, other).wait_recv()
 
     def to_other(rel, k):
         at = xbuf.at[c, slot(k, rel), :, body]
-        return rc(at, at, s_p.at[k * n_sp + rel], r_p.at[k * n_sp + rel], other)
+        return rc(at, at, s_p, r_p.at[k * n_sp + rel], other)
 
 
     def ap_copy(rel):
         at = xbuf.at[c, z * n_sp + sp, :, along]
-        return rc(at, at, s_ap.at[rel], r_ap.at[rel], (columns[rel], tp))
+        return rc(at, at, s_ap, r_ap.at[rel], (columns[rel], tp))
 
     def ap_recv(rel):
         at = xbuf.at[c, slot(0, rel), :, along]
-        return rc(at, at, s_ap.at[rel], r_ap.at[rel], (columns[rel], tp))
+        return rc(at, at, s_ap, r_ap.at[rel], (columns[rel], tp))
 
     def az_copy(k):
         at = xbuf.at[c, pl.ds(z * n_sp, n_sp), :, along]
-        return rc(at, at, s_az.at[k], r_az.at[z], (sp, zz(k) * 2 + c))
+        return rc(at, at, s_az, r_az.at[z], (sp, zz(k) * 2 + c))
 
     def az_recv(k):
         at = xbuf.at[c, group(k), :, along]
-        return rc(at, at, s_az.at[k], r_az.at[zz(k)], (sp, zz(k) * 2 + c))
+        return rc(at, at, s_az, r_az.at[zz(k)], (sp, zz(k) * 2 + c))
 
     def ao_copy(k):
         at = xbuf.at[c, group(k), :, along]
-        return rc(at, at, s_ao.at[k], r_ao.at[k], other)
+        return rc(at, at, s_ao, r_ao.at[k], other)
 
     def spread(k):
         for h in (1, 0):
@@ -303,7 +301,7 @@
 
     def d_copy(s):
         i = couple(zz(s // 2), s)
-        return rc(pbuf.at[1 - c, i], dbuf.at[i], s_d.at[s], r_d.at[s], other)
+        return rc(pbuf.at[1 - c, i], dbuf.at[i], s_d, r_d.at[s], other)
 
     def merge(s):
         d_copy(s).wait_recv()
@@ -316,11 +314,11 @@
     def r1_copy(h, o, k):
         rel = DG if o else (XN if h == 0 else YN)
         at = pbuf.at[c, slot(k, rel), :, part(h)]
-        return rc(at, r1.at[h, o, k], s_r1.at[h, o, k], r_r1.at[h, o, k], to_x if h == 0 else to_y)
+        return rc(at, r1.at[h, o, k], s_r1, r_r1.at[h, o, k], to_x if h == 0 else to_y)
 
     def r2_copy(h, k):
         at = pbuf.at[c, slot(k, YN if h == 0 else XN), :, part(h)]
-        return rc(at, r2.at[h, k], s_r2.at[h, k], r_r2.at[h, k], to_y if h == 0 else to_x)
+        return rc(at, r2.at[h, k], s_r2, r_r2.at[h, k], to_y if h == 0 else to_x)
 
     def mate_copy(h, k):
         at = pbuf.at[c, slot(k, OWN), :, part(h)]
@@ -333,18 +331,18 @@
 
     def bz_copy(k):
         return rc(
-            pbuf.at[c, group(k), :, along], rbz.at[z], s_bz.at[k], r_bz.at[z], (sp, zz(k) * 2 + c)
+            pbuf.at[c, group(k), :, along], rbz.at[z], s_bz, r_bz.at[z], (sp, zz(k) * 2 + c)
         )
 
     def bz_recv(k):
         return rc(
-            pbuf.at[c, group(k), :, along], rbz.at[zz(k)], s_bz.at[k], r_bz.at[zz(k)],
+            pbuf.at[c, group(k), :, along], rbz.at[zz(k)], s_bz, r_bz.at[zz(k)],
             (sp, zz(k) * 2 + c),
         )
 
     def bp_copy(rel):
         return rc(
-            pbuf.at[c, slot(0, rel), :, along], rbp.at[rel], s_bp.at[rel], r_bp.at[rel],
+            pbuf.at[c, slot(0, rel), :, along], rbp.at[rel], s_bp, r_bp.at[rel],
             (columns[rel], tp),
         )
 
@@ -503,12 +501,12 @@
             column = jnp.where(side == 0, columns[b], columns[2 + b])
             at = xbuf.at[1 - c, at_z * n_sp + column, :, body]
             n = k * n_sp + 2 * side + b
-            rc(at, at, s_p.at[n], r_p.at[n], other).wait_recv()
+            rc(at, at, s_p, r_p.at[n], other).wait_recv()
 
         @pl.when(side == 0)
         def _():
             at = xbuf.at[1 - c, pl.ds(at_z * n_sp, n_sp), :, along]
-            rc(at, at, s_ao.at[k], r_ao.at[k], other).wait_recv()
+            rc(at, at, s_ao, r_ao.at[k], other).wait_recv()
 
         i = couple(at_z, s)
         held = xbuf[:, i].reshape(4 * rows, width)
@@ -540,7 +538,7 @@
 
         down = jnp.dot(acts[...], wd[...], preferred_element_type=f32)
         pbuf[:, i] = down.astype(pbuf.dtype).reshape(2, 2, rows, width)
-        rc(pbuf.at[1 - c, i], dbuf.at[i], s_d.at[s], r_d.at[s], other).start()
+        rc(pbuf.at[1 - c, i], dbuf.at[i], s_d, r_d.at[s], other).start()
 
         for at, works in after.items():
             @pl.when(s == at)
@@ -575,29 +573,11 @@
 
     for copy in halo_copies():
         copy.wait_send()
-    for d in range(1, n_tp):
-        @pl.when(lax.rem(tp + d, n_tp) != 0)
-        def _():
-            swap(d).wait_send()
-
-    @pl.when(tp != 0)
-    def _():
-        swap_first().wait_send()
-
-    for rel in (XN, YN, DG):
-        name_copy(rel).wait_send()
-        bp_copy(rel).wait_send()
-        ap_copy(rel).wait_send()
-    for k in range(1, nz):
-        bz_copy(k).wait_send()
-        az_copy(k).wait_send()
-    for k in range(nz):
-        ao_copy(k).wait_send()
-    for d in range(1, n_tp):
-        table_copy(d).wait_send()
-    z_send(1).wait_send()
+    swaps().wait_send()
+    tables().wait_send()
     for h in (0, 1):
         rz_copy(h, 1).wait_send()
+    z_send(1).wait_send()
 
     @pl.when(inner)
     def _():
@@ -614,18 +594,22 @@
             for h in (0, 1):
                 mate_copy(h, k).wait_send()
 
-    for k in range(nz):
-        for h in (0, 1):
-            first(h, k).wait_send()
-            second(h, k).wait_send()
-            third(h, k).wait_send()
-            r1_copy(h, 0, k).wait_send()
-            r1_copy(h, 1, k).wait_send()
-            r2_copy(h, k).wait_send()
-        for rel in range(n_sp):
-            to_other(rel, k).wait_send()
-    for s in range(steps):
-        d_copy(s).wait_send()
+    def sent(at, ss):
+        rc(at, at, ss, r_t, other).wait_send()
+
+    every = nz * n_sp
+    sent(named.at[pl.ds(0, n_sp - 1)], s_n)
+    sent(xbuf.at[c, pl.ds(0, 2 * nz), :, part(0)], s_1)
+    sent(xbuf.at[c, pl.ds(0, every), :, part(0)], s_2)
+    sent(xbuf.at[c, pl.ds(0, every), :, body], s_p)
+    sent(xbuf.at[c, pl.ds(0, n_sp - 1), :, along], s_ap)
+    sent(xbuf.at[c, pl.ds(0, every - n_sp), :, along], s_az)
+    sent(xbuf.at[c, pl.ds(0, every), :, along], s_ao)
+    sent(pbuf.at[c], s_d)
+    sent(pbuf.at[c, pl.ds(0, every), :, part(0)], s_r1)
+    sent(pbuf.at[c, pl.ds(0, 2 * nz), :, part(0)], s_r2)
+    sent(pbuf.at[c, pl.ds(0, every - n_sp), :, along], s_bz)
+    sent(rbp.at[pl.ds(0, n_sp - 1)], s_bp)
 
 
 def layer(gate_b, gate_c, values_in, conv_w, docs, resid, gain, ids, route, w_out, w_gate, w_up, w_down):
@@ -676,15 +660,11 @@
             pltpu.VMEM(w_up.shape, bf),
             pltpu.VMEM(w_down.shape, bf),
             dma((9,)), dma((4,)),
-            dma((n_tp,)), dma((n_tp,)), dma, dma((3,)), dma((3,)),
-            dma((4,)), dma((4,)), dma((n_tp,)), dma((n_tp,)),
-            dma((nz,)), dma((nz,)), dma((nz,)), dma((2, nz)), dma((2, 2, nz)), dma((2, 4, nz)),
-            dma((n_sp * nz,)), dma((n_sp * nz,)),
-            dma((2 * nz,)), dma((2 * nz,)),
-            dma((2, 2, nz)), dma((2, 2, nz)), dma((2, nz)), dma((2, nz)),
+            dma, dma, dma((3,)), dma((3,)), dma, dma((4,)), dma, dma,
+            dma((nz,)), dma((nz,)), dma((nz,)), dma, dma, dma((2, 4, nz)), dma, dma((n_sp * nz,)),
+            dma, dma((2 * nz,)), dma, dma((2, 2, nz)), dma, dma((2, nz)),
             dma((2, 2)), dma((2, 2)), dma((nz, 2)), dma((2, 2)),
-            dma((nz,)), dma((nz,)), dma((4,)), dma((4,)),
-            dma((4,)), dma((4,)), dma((nz,)), dma((nz,)), dma((nz,)), dma((nz,)),
+            dma, dma((nz,)), dma, dma((4,)), dma, dma((4,)), dma, dma((nz,)), dma, dma((nz,)),
         ],
         compiler_params=pltpu.CompilerParams(
             collective_id=0, has_side_effects=True, vmem_limit_bytes=64000000

time: 87.9 us -> 86.8 us (0.987)
  Pallas kernels: 87.1 us -> 85.9 us
    pallas_call x1, Pallas kernels: 87.1 us -> 85.9 us  [layer(): pl.pallas_call(moe_kernel, out_shape=pltpu.VMEM((rows, width), bf), in_sp...]
where the time goes in v4:
time: 86.8 us; the launch traced here: 86.7 us
  Pallas kernels  85.9 us (99%)
    pallas_call x1, Pallas kernels, layer(): pl.pallas_call(moe_kernel, out_shape=pltpu.VMEM((rows, width), bf), in_sp...  85.9 us

profile of v4, /device:TPU:0, one launch (start us, length us, event | category | flops | bytes accessed | tf_op | source)
XLA Modules:
  0.0 86.7 jit_solution(2105553579652209495)
XLA Ops:
  0.0 85.9 %shard_map.127 = bf16[64,2048]{1,0:T(8,128)(2,1)S(1)} custom-call(bf16[512,128]{1,0:T(8,128)(2,1)} %gb_hbm.1, bf16[512,128]{1,0:T(8,128)(2,1)} %gc_hbm.1, bf16[512,128]{1,0:T(8,128)(2,1)} %vals_hbm.1, bf16[3,128]{1,0:T(4,128)(2,1)} %taps_hbm.1, s32[4,128]{1,0:T(4,128)} %bitcast.11, bf16[64,2048]{1,0:T(8,128)(2,1)} %resid_hbm.1, bf16[16,128]{1,0:T(8,128)(2,1)} %bitcast.10, ...), custom_call_target="tpu_custom_call" | custom-call | tf_op jit(solution)/shard_map/pallas_call | solution.py:629
  86.0 0.7 copy.15

commit v5 on v4

--- a/solution.py
+++ b/solution.py
@@ -467,7 +467,7 @@
     end = nz - 1
     put(before, 1, relay, 1)
     put(middle, 0, corner, 0)
-    put(middle, 1, pass_on, end)
+    put(before, 2, pass_on, end)
     for k in range(1, nz):
         if k < end:
             put(middle, 2 * k - 1, take, k + 1)

time: 86.8 us -> 85.5 us (0.985)
  Pallas kernels: 85.9 us -> 84.7 us
    pallas_call x1, Pallas kernels: 85.9 us -> 84.7 us  [layer(): pl.pallas_call(moe_kernel, out_shape=pltpu.VMEM((rows, width), bf), in_sp...]
where the time goes in v5:
time: 85.5 us; the launch traced here: 85.4 us
  Pallas kernels  84.7 us (99%)
    pallas_call x1, Pallas kernels, layer(): pl.pallas_call(moe_kernel, out_shape=pltpu.VMEM((rows, width), bf), in_sp...  84.7 us

profile of v5, /device:TPU:0, one launch (start us, length us, event | category | flops | bytes accessed | tf_op | source)
XLA Modules:
  0.0 85.4 jit_solution(5806789094504425583)
XLA Ops:
  0.0 84.7 %shard_map.127 = bf16[64,2048]{1,0:T(8,128)(2,1)S(1)} custom-call(bf16[512,128]{1,0:T(8,128)(2,1)} %gb_hbm.1, bf16[512,128]{1,0:T(8,128)(2,1)} %gc_hbm.1, bf16[512,128]{1,0:T(8,128)(2,1)} %vals_hbm.1, bf16[3,128]{1,0:T(4,128)(2,1)} %taps_hbm.1, s32[4,128]{1,0:T(4,128)} %bitcast.11, bf16[64,2048]{1,0:T(8,128)(2,1)} %resid_hbm.1, bf16[16,128]{1,0:T(8,128)(2,1)} %bitcast.10, ...), custom_call_target="tpu_custom_call" | custom-call | tf_op jit(solution)/shard_map/pallas_call | solution.py:629
  84.7 0.7 copy.15
